TPU v7x, 32 devices: a whole 2x2x4 slice. The times are simulated.
32 devices in a mesh: sp: 4 (over z), tp: 4 (over y, x), dp: 2 (over core).
Axes of the slice: x: 2, y: 2, z: 4, core: 2. Of those that a mesh axis runs over, the one named last changes fastest.
Arguments:
- latent: bfloat16 [2, 512, 2048], P('dp', ('sp', 'tp')), may hold values from -10 to 10
- condition: bfloat16 [2, 2048], P('dp'), may hold values from -6 to 6
- context: bfloat16 [2, 512, 2048], P('dp', 'sp'), may hold values from -6 to 6
- context_source: bfloat16 [2048], replicated, may hold values from -6 to 6
- mod_weight: bfloat16 [3, 2048, 2048], P(None, 'sp', 'tp'), may hold values from -0.125 to 0.125
- norm_gain: bfloat16 [2048], replicated, may hold values from 0.099609375 to 1.8984375
- w_x: bfloat16 [2048, 2048], P('dp', 'tp'), may hold values from -0.125 to 0.125
- w_b: bfloat16 [2048, 512], P('dp', 'tp'), may hold values from -0.125 to 0.125
- w_c: bfloat16 [2048, 512], P('dp', 'tp'), may hold values from -0.125 to 0.125
- w_z: bfloat16 [2048, 2048], P('dp', 'tp'), may hold values from -0.125 to 0.125
- w_dt: bfloat16 [2, 2048, 32], P(None, 'dp', 'tp'), may hold values from -0.125 to 0.125
- conv_x: bfloat16 [3, 2048], P(None, 'tp'), may hold values from -3.5 to 3.5
- conv_b: bfloat16 [3, 512], P(None, 'tp'), may hold values from -3.5 to 3.5
- conv_c: bfloat16 [3, 512], P(None, 'tp'), may hold values from -3.5 to 3.5
- decay_rate: float32 [2, 32], P(None, 'tp'), may hold values from 0 to 1, as said below
- out_gain: bfloat16 [2048], P('tp'), may hold values from 0.099609375 to 1.8984375
- w_out: bfloat16 [2048, 2048], P(('tp', 'dp')), may hold values from -0.125 to 0.125
Outputs:
- update: bfloat16 [2, 512, 2048], P('dp', ('sp', 'tp'))
Inputs may be any that keep to these rules, and one draw needn't show every extreme that they name: `decay_rate`: positive rates.
All inputs are finite; a program needn't handle non-finite values.
Results may differ from a plain program's by a relative error of at most 0.014.
Values may be sent and summed in bfloat16 or wider, within the bound.
A program may use at most 128 MiB of HBM per device.

v0:
```python
import jax
import jax.numpy as jnp
from jax import lax
from jax.sharding import PartitionSpec as P

STATE = 128
BLOCK = 128


EPSILON = 1e-06


def with_halo(x, sides, width):
    for axis, dim in sides:
        peers, length = (lax.axis_size(axis), x.shape[dim])
        up = [(i, (i + 1) % peers) for i in range(peers - 1)]
        down = [(j, i) for i, j in up]
        last = lax.slice_in_dim(x, length - width, length, axis=dim)
        leading = lax.slice_in_dim(x, 0, width, axis=dim)
        before = lax.ppermute(last, axis, up)
        after = lax.ppermute(leading, axis, down)
        x = jnp.concatenate([before, x, after], axis=dim)
    return x


def carried_in_2(x, axis, combine, identity, reverse):
    peers, place = (lax.axis_size(axis), lax.axis_index(axis))
    everything = jax.tree.map(
        lambda part, kind: lax.all_gather(part.astype(kind), axis), x, (jnp.bfloat16, jnp.bfloat16)
    )
    start = jax.tree.map(
        lambda part, zero: jnp.broadcast_to(jnp.asarray(zero, part.dtype), part.shape), x, identity
    )

    def hop(k, before):
        at = peers - 1 - k if reverse else k
        reached = at > place if reverse else at < place
        new = combine(
            before, jax.tree.map(lambda part, own: part[at].astype(own.dtype), everything, x)
        )
        return jax.tree.map(lambda a, b: jnp.where(reached, a, b), new, before)

    return lax.fori_loop(0, peers, hop, start)


def rounded(values):
    return lax.optimization_barrier(values.astype(jnp.bfloat16)).astype(jnp.float32)


def modulated(source, gain_vec, shift_vec, scale_vec):
    values = source.astype(jnp.float32)
    normed = values * lax.rsqrt(jnp.mean(values * values, axis=-1, keepdims=True) + EPSILON)
    return (normed * gain_vec.astype(jnp.float32) * (1.0 + scale_vec) + shift_vec).astype(
        jnp.bfloat16
    )


def convolved(padded, weight, total_rows):
    wide_vals = padded.astype(jnp.float32)
    tap_weights = weight.astype(jnp.float32)
    summed = jnp.zeros((total_rows, wide_vals.shape[1]), jnp.float32)
    for offset in range(weight.shape[0]):
        summed = summed + wide_vals[offset : offset + total_rows] * tap_weights[offset]
    return jax.nn.silu(summed).astype(jnp.bfloat16)


def final_state(x_vals, b_vals, step_size, rate_head, groups):
    total_rows, head_count = step_size.shape
    per_group = head_count // groups
    moved_x = rounded(
        x_vals.reshape(total_rows, head_count, -1).astype(jnp.float32) * step_size[:, :, None]
    )
    running = jnp.cumsum(-rate_head * step_size, axis=0)
    weight = jnp.exp(running[-1:] - running)
    scaled = (moved_x * weight[:, :, None]).reshape(total_rows, groups, per_group, -1)
    b_wide = b_vals.reshape(total_rows, groups, -1).astype(jnp.float32)
    ctx_state = jnp.einsum("sgn,sghp->ghpn", b_wide, scaled, precision=lax.Precision.HIGHEST)
    return (ctx_state, running[-1].reshape(groups, per_group))


def combine_states(earlier, later_part):
    return (
        earlier[0] + later_part[0],
        earlier[1] * jnp.exp(later_part[0])[:, :, None, None] + later_part[1],
    )


def direction_terms(x_vals, b_vals, c_vals, step_size, rate_head, groups):
    total_rows, head_count = step_size.shape
    per_group = head_count // groups
    blocks = total_rows // BLOCK
    moved_x = (
        x_vals.reshape(total_rows, head_count, -1).astype(jnp.float32) * step_size[:, :, None]
    ).astype(jnp.bfloat16)
    head_dim = moved_x.shape[2]
    x_blocks = moved_x.reshape(blocks, BLOCK, groups, per_group, head_dim)
    b_blocks = b_vals.reshape(blocks, BLOCK, groups, -1)
    c_blocks = c_vals.reshape(blocks, BLOCK, groups, -1)
    running = jnp.cumsum((-rate_head * step_size).reshape(blocks, BLOCK, head_count), axis=1)
    across = jnp.swapaxes(running, 1, 2)
    spread = across[:, :, :, None] - across[:, :, None, :]
    lower_part = lax.broadcasted_iota(jnp.int32, (BLOCK, BLOCK), 0) >= lax.broadcasted_iota(
        jnp.int32, (BLOCK, BLOCK), 1
    )
    decay_mask = jnp.where(lower_part, jnp.exp(jnp.minimum(spread, 0.0)), 0.0).reshape(
        blocks, groups, per_group, BLOCK, BLOCK
    )
    scores = jnp.einsum("clgn,csgn->cgls", c_blocks, b_blocks, preferred_element_type=jnp.float32)
    weights = (scores[:, :, None] * decay_mask).astype(jnp.bfloat16)
    inside = jnp.einsum("cghls,csghp->clghp", weights, x_blocks, preferred_element_type=jnp.float32)
    to_end = jnp.exp(running[:, -1:, :] - running).reshape(blocks, BLOCK, groups, per_group, 1)
    x_end = (x_blocks.astype(jnp.float32) * to_end).astype(jnp.bfloat16)
    fresh_state = jnp.einsum(
        "csgn,csghp->cghpn", b_blocks, x_end, preferred_element_type=jnp.float32
    )
    totals = running[:, -1, :].reshape(blocks, groups, per_group)

    def advance(carried_in, inputs):
        return (carried_in * jnp.exp(inputs[1])[:, :, None, None] + inputs[0], carried_in)

    ending, before = lax.scan(
        advance, jnp.zeros(fresh_state.shape[1:], jnp.float32), (fresh_state, totals)
    )
    return (inside, before, ending, totals, running, c_blocks)


def direction_output(terms, incoming):
    inside, before, ending, totals, running, c_blocks = terms
    blocks, length, groups, per_group, head_dim = inside.shape
    offset_sum = jnp.cumsum(totals, axis=0) - totals
    entering = before + jnp.exp(offset_sum)[:, :, :, None, None] * incoming[None]
    carried = jnp.einsum(
        "clgn,cghpn->clghp",
        c_blocks,
        entering.astype(jnp.bfloat16),
        preferred_element_type=jnp.float32,
    )
    growth = jnp.exp(running).reshape(blocks, length, groups, per_group, 1)
    return (inside + growth * carried).reshape(blocks * length, -1)


def shards(
    latent,
    condition,
    context,
    context_source,
    mod_weight,
    norm_gain,
    w_x,
    w_b,
    w_c,
    w_z,
    w_dt,
    conv_x,
    conv_b,
    conv_c,
    decay_rate,
    out_gain,
    w_out,
):
    row_count = mod_weight.shape[1]
    activations = jnp.stack(
        [
            jax.nn.silu(condition[0].astype(jnp.float32)),
            jax.nn.silu(context_source.astype(jnp.float32)),
        ]
    ).astype(jnp.bfloat16)
    own_rows = lax.dynamic_slice_in_dim(activations, lax.axis_index("sp") * row_count, row_count, 1)
    partial_value = jnp.einsum(
        "ar,krc->kac", own_rows, mod_weight, preferred_element_type=jnp.float32
    )
    summed = lax.psum(partial_value, "sp")
    mod_vectors = lax.all_gather(summed, "tp", axis=2, tiled=True)
    full_x, full_b, full_c, full_z, full_fwd, full_bwd, full_out = (
        lax.all_gather(w_x, "dp", axis=0, tiled=True),
        lax.all_gather(w_b, "dp", axis=0, tiled=True),
        lax.all_gather(w_c, "dp", axis=0, tiled=True),
        lax.all_gather(w_z, "dp", axis=0, tiled=True),
        lax.all_gather(w_dt[0], "dp", axis=0, tiled=True),
        lax.all_gather(w_dt[1], "dp", axis=0, tiled=True),
        lax.all_gather(w_out, "dp", axis=0, tiled=True),
    )
    inner_cols = full_x.shape[1]
    gn_cols = full_b.shape[1]
    head_count = full_fwd.shape[1]
    groups = gn_cols // STATE
    mixed_cols = inner_cols + gn_cols
    reach_rows = conv_x.shape[0] // 2
    rate_fwd = decay_rate[0]
    rate_bwd = decay_rate[1]
    all_weights = jnp.concatenate([full_x, full_b, full_c, full_fwd, full_bwd, full_z], axis=1)
    ctx_weight = jnp.concatenate([full_x, full_b, full_fwd, full_bwd], axis=1)
    taps_all = jnp.concatenate([conv_x, conv_b, conv_c], axis=1)
    ctx_taps = jnp.concatenate([conv_x, conv_b], axis=1)
    ctx_rows = modulated(context[0], norm_gain, mod_vectors[0, 1], mod_vectors[1, 1])
    own_features = jnp.dot(ctx_rows, ctx_weight, preferred_element_type=jnp.float32).astype(
        jnp.bfloat16
    )
    own_count = own_features.shape[0]
    padded = with_halo(own_features[:, :mixed_cols], (("sp", 0),), reach_rows)
    smoothed = convolved(padded, ctx_taps, own_count)
    step_size = jax.nn.softplus(own_features[:, mixed_cols:].astype(jnp.float32))
    ctx_x = smoothed[:, :inner_cols]
    ctx_b = smoothed[:, inner_cols:]
    part_fwd, total_fwd = final_state(ctx_x, ctx_b, step_size[:, :head_count], rate_fwd, groups)
    part_bwd, total_bwd = final_state(
        jnp.flip(ctx_x, 0),
        jnp.flip(ctx_b, 0),
        jnp.flip(step_size[:, head_count:], 0),
        rate_bwd,
        groups,
    )
    totals = lax.all_gather(jnp.stack([total_fwd, total_bwd])[None], "sp", axis=0, tiled=True)
    device_order = jnp.arange(totals.shape[0])
    own_index = lax.axis_index("sp")
    after_sum = jnp.sum(
        jnp.where((device_order > own_index)[:, None, None], totals[:, 0], 0.0), axis=0
    )
    before_sum = jnp.sum(
        jnp.where((device_order < own_index)[:, None, None], totals[:, 1], 0.0), axis=0
    )
    ctx_fwd, ctx_bwd = lax.psum(
        (
            part_fwd * jnp.exp(after_sum)[:, :, None, None],
            part_bwd * jnp.exp(before_sum)[:, :, None, None],
        ),
        "sp",
    )
    latent_rows = modulated(latent[0], norm_gain, mod_vectors[0, 0], mod_vectors[1, 0])
    features = jnp.dot(
        lax.all_gather(latent_rows, "tp", axis=0, tiled=True),
        all_weights,
        preferred_element_type=jnp.float32,
    ).astype(jnp.bfloat16)
    total_rows = features.shape[0]
    padded = with_halo(features[:, : mixed_cols + gn_cols], (("sp", 0),), reach_rows)
    smoothed = convolved(padded, taps_all, total_rows)
    x_vals = smoothed[:, :inner_cols]
    b_vals = smoothed[:, inner_cols:mixed_cols]
    c_vals = smoothed[:, mixed_cols:]
    base_col = mixed_cols + gn_cols
    step_size = jax.nn.softplus(
        features[:, base_col : base_col + 2 * head_count].astype(jnp.float32)
    )
    gate_in = features[:, base_col + 2 * head_count :]
    forward_terms = direction_terms(
        x_vals, b_vals, c_vals, step_size[:, :head_count], rate_fwd, groups
    )
    backward_terms = direction_terms(
        jnp.flip(x_vals, 0),
        jnp.flip(b_vals, 0),
        jnp.flip(c_vals, 0),
        jnp.flip(step_size[:, head_count:], 0),
        rate_bwd,
        groups,
    )
    fwd_total = jnp.sum(forward_terms[3], axis=0)
    bwd_total = jnp.sum(backward_terms[3], axis=0)
    empty = (jnp.zeros_like(fwd_total), jnp.zeros_like(forward_terms[2]))
    prefix_decay, prefix_state = carried_in_2(
        (fwd_total, forward_terms[2]), "sp", combine_states, empty, False
    )
    suffix_decay, suffix_state = carried_in_2(
        (bwd_total, backward_terms[2]), "sp", combine_states, empty, True
    )
    out_fwd = direction_output(
        forward_terms, prefix_state + jnp.exp(prefix_decay)[:, :, None, None] * ctx_fwd
    )
    out_bwd = jnp.flip(
        direction_output(
            backward_terms, suffix_state + jnp.exp(suffix_decay)[:, :, None, None] * ctx_bwd
        ),
        0,
    )
    gated = (out_fwd + out_bwd) * jax.nn.silu(gate_in.astype(jnp.float32))
    grouped = gated.reshape(total_rows, groups, -1)
    normed = (
        grouped
        * lax.rsqrt(jnp.mean(grouped * grouped, axis=-1, keepdims=True) + EPSILON)
        * out_gain.reshape(groups, -1).astype(jnp.float32)
    )
    normed_out = normed.reshape(total_rows, -1).astype(jnp.bfloat16)
    mixed = lax.psum_scatter(
        jnp.dot(normed_out, full_out, preferred_element_type=jnp.float32).astype(jnp.bfloat16),
        "tp",
        scatter_dimension=0,
        tiled=True,
    ).astype(jnp.float32)
    return (mod_vectors[2, 0] * mixed).astype(jnp.bfloat16)[None]


def solution(mesh):
    placed = (
        P("dp", ("sp", "tp"), None),
        P("dp", None),
        P("dp", "sp", None),
        P(),
        P(None, "sp", "tp"),
        P(),
        P("dp", "tp"),
        P("dp", "tp"),
        P("dp", "tp"),
        P("dp", "tp"),
        P(None, "dp", "tp"),
        P(None, "tp"),
        P(None, "tp"),
        P(None, "tp"),
        P(None, "tp"),
        P("tp"),
        P(("tp", "dp"), None),
    )
    return jax.shard_map(
        shards, mesh=mesh, in_specs=placed, out_specs=P("dp", ("sp", "tp"), None), check_vma=False
    )
```

profile of v0, /device:TPU:0, one launch (start us, length us, event | category | flops | bytes accessed | tf_op | source)
XLA Modules:
  0.0 216.8 jit_solution(12759376264633219292)
XLA Ops:
  6.6 0.7 all-gather.9.cloned.1.call-update
  7.3 0.7 all-gather.11.cloned.1.call-update
  8.1 0.7 fusion.91
  8.8 0.7 fusion.100
  9.9 20.4 %psum.21 = f32[3,2,512]{2,1,0:T(2,128)S(1)} all-reduce(f32[3,2,512]{2,1,0:T(2,128)S(1)} %convolution_bitcast_fusion.4), channel_id=1, replica_groups=mesh['sp'=4,'tp'=4,'dp'=2] {'sp'}, use_global_device_ids=true, to_apply=%region_0.1 | all-reduce | flops 3072 | bytes 24576 | tf_op jit(solution)/shard_map/psum | solution.py:172
  30.4 8.3 %all_gather.50 = f32[3,2,2048]{2,1,0:T(2,128)S(1)} all-gather(f32[3,2,512]{2,1,0:T(2,128)S(1)} %psum.21), channel_id=1, replica_groups=mesh['sp'=4,'tp'=4,'dp'=2] {'tp'}, dimensions={2}, use_global_device_ids=true | all-gather | bytes 61440 | tf_op jit(solution)/shard_map/all_gather | solution.py:173
  39.1 1.8 all-gather
  41.2 1.8 all-gather.1
  43.3 10.0 %all_gather.51 = bf16[128,2048]{1,0:T(8,128)(2,1)S(1)} all-gather(bf16[32,2048]{1,0:T(8,128)(2,1)S(1)} %fusion.46), channel_id=1, replica_groups=mesh['sp'=4,'tp'=4,'dp'=2] {'tp'}, dimensions={0}, use_global_device_ids=true | all-gather | bytes 655360 | tf_op jit(solution)/shard_map/all_gather | solution.py:231
  53.9 3.8 %all_gather.53 = bf16[2048,128]{1,0:T(8,128)(2,1)} all-gather(bf16[1024,128]{1,0:T(8,128)(2,1)} %param.28), channel_id=1, replica_groups=mesh['sp'=4,'tp'=4,'dp'=2] {'dp'}, dimensions={0}, use_global_device_ids=true | all-gather | bytes 786432 | tf_op jit(solution)/shard_map/all_gather | solution.py:176
  57.7 4.1 %all_gather.54 = bf16[2048,128]{1,0:T(8,128)(2,1)} all-gather(bf16[1024,128]{1,0:T(8,128)(2,1)} %param.29), channel_id=1, replica_groups=mesh['sp'=4,'tp'=4,'dp'=2] {'dp'}, dimensions={0}, use_global_device_ids=true | all-gather | bytes 786432 | tf_op jit(solution)/shard_map/all_gather | solution.py:177
  61.8 1.2 fusion.23
  63.0 3.5 %fusion.16 = bf16[128,656]{0,1:T(8,128)(2,1)S(1)} fusion(bf16[2048,8]{1,0:T(8,128)(2,1)S(1)} %copy.71, bf16[2048,8]{1,0:T(8,128)(2,1)S(1)} %copy.70, bf16[2048,128]{1,0:T(8,128)(2,1)} %all_gather.53, bf16[2048,512]{1,0:T(8,128)(2,1)} %all-gather.9.cloned.1.call-done, bf16[1,128,2048]{2,1,0:T(8,128)(2,1)} %param.23, f32[2048]{0:T(1024)S(1)} %bitcast.220, ...), kind=kOutput, calls=%fused_computation.38 | convolution fusion | flops 356337664 | bytes 3404288 | tf_op jit(solution)/shard_map/dot_general | solution.py:196
  66.6 0.8 fusion.124
  67.4 10.2 %concatenate.18 = bf16[2048,1296]{1,0:T(8,128)(2,1)} concatenate(bf16[2048,512]{1,0:T(8,128)(2,1)} %all-gather.9.cloned.1.call-done, bf16[2048,128]{1,0:T(8,128)(2,1)} %all_gather.53, bf16[2048,128]{1,0:T(8,128)(2,1)} %all_gather.54, bf16[2048,8]{1,0:T(8,128)(2,1)S(1)} %copy.70, bf16[2048,8]{1,0:T(8,128)(2,1)S(1)} %copy.71, bf16[2048,512]{1,0:T(8,128)(2,1)} %all-gather.11.cloned.1.call-done), dimensions={1} | concatenate | bytes 10616832 | tf_op jit(solution)/shard_map/concatenate | solution.py:191
  77.6 5.0 %convolution_convert_fusion.1 = bf16[128,1296]{0,1:T(8,128)(2,1)S(1)} fusion(bf16[128,2048]{1,0:T(8,128)(2,1)S(1)} %all_gather.51, bf16[2048,1296]{1,0:T(8,128)(2,1)} %concatenate.18), kind=kOutput, calls=%fused_computation.23 | convolution fusion | flops 679643136 | bytes 6164480 | tf_op jit(solution)/shard_map/dot_general | solution.py:230
  84.0 7.6 %all-gather.3 = f32[8,1,8]{2,1,0:T(1,128)S(1)} all-gather(f32[2,1,8]{2,1,0:T(1,128)S(1)} %pad_maximum_fusion.3), channel_id=5, replica_groups=mesh['sp'=4,'tp'=4,'dp'=2] {'sp'}, dimensions={0}, use_global_device_ids=true | all-gather | bytes 320 | tf_op jit(solution)/shard_map/all_gather | solution.py:213
  91.7 3.9 %collective-permute-start.2 = (bf16[1,640]{0,1:T(8,128)(2,1)S(1)}, bf16[1,640]{0,1:T(8,128)(2,1)S(1)}, u32[]{:S(2)}, u32[]{:S(2)}) collective-permute-start(bf16[1,640]{0,1:T(8,128)(2,1)S(1)} %copy-done.5), channel_id=1, source_target_pairs={{0,8},{8,16},{16,24},{1,9},{9,17},{17,25},{2,10},{10,18},{18,26},{... | collective-permute-start | bytes 3848 | tf_op jit(solution)/shard_map/ppermute | solution.py:20
  95.6 1.3 collective-permute-start.3
  97.2 1.1 collective-permute-done.2
  98.4 4.4 %collective-permute-done.3 = bf16[1,640]{0,1:T(8,128)(2,1)S(1)} collective-permute-done((bf16[1,640]{0,1:T(8,128)(2,1)S(1)}, bf16[1,640]{0,1:T(8,128)(2,1)S(1)}, u32[]{:S(2)}, u32[]{:S(2)}) %collective-permute-start.3) | collective-permute-done | bytes 1312 | tf_op jit(solution)/shard_map/ppermute | solution.py:21
  104.1 1.0 fusion.14
  105.1 1.0 fusion.12
  106.8 0.6 iota_compare_fusion
  107.4 0.6 convert_reduce_fusion.1
  111.0 1.9 collective-permute-start
  113.0 1.3 collective-permute-start.1
  114.3 0.7 bitcast_exponential_fusion.1
  114.9 0.7 bitcast_exponential_fusion
  116.1 11.0 %all_gather.58 = bf16[4,1,8]{2,1,0:T(2,128)(2,1)} all-gather(bf16[1,1,8]{2,1,0:T(2,128)(2,1)S(1)} %slice.299), channel_id=1, replica_groups=mesh['sp'=4,'tp'=4,'dp'=2] {'sp'}, dimensions={0}, use_global_device_ids=true | all-gather | bytes 80 | tf_op jit(solution)/shard_map/all_gather | solution.py:29
  127.2 10.0 %all_gather.62 = bf16[4,1,8]{2,1,0:T(2,128)(2,1)} all-gather(bf16[1,1,8]{2,1,0:T(2,128)(2,1)S(1)} %slice.298), channel_id=1, replica_groups=mesh['sp'=4,'tp'=4,'dp'=2] {'sp'}, dimensions={0}, use_global_device_ids=true | all-gather | bytes 80 | tf_op jit(solution)/shard_map/all_gather | solution.py:29
  137.2 0.7 copy.73
  137.8 0.7 copy.86
  138.8 1.3 multiply_convert_fusion.2
  140.1 0.7 slice_convert_fusion.2
  141.1 15.0 %all-gather.2 = bf16[32,64,128]{2,1,0:T(8,128)(2,1)S(1)} all-gather(bf16[8,64,128]{2,1,0:T(8,128)(2,1)S(1)} %fusion.21), channel_id=4, replica_groups=mesh['sp'=4,'tp'=4,'dp'=2] {'sp'}, dimensions={0}, use_global_device_ids=true | all-gather | bytes 655360 | tf_op jit(solution)/shard_map/all_gather | solution.py:29
  156.1 0.7 while.44
  158.3 15.8 %all-gather.4 = bf16[32,64,128]{2,1,0:T(8,128)(2,1)S(1)} all-gather(bf16[8,64,128]{2,1,0:T(8,128)(2,1)S(1)} %fusion.22), channel_id=6, replica_groups=mesh['sp'=4,'tp'=4,'dp'=2] {'sp'}, dimensions={0}, use_global_device_ids=true | all-gather | bytes 655360 | tf_op jit(solution)/shard_map/all_gather | solution.py:29
  174.1 0.7 while.45
  174.8 0.8 fusion.117
  175.6 0.8 fusion.131
  176.4 1.2 fusion.20
  177.6 1.2 fusion.13
  179.2 1.2 fusion.19
  180.4 1.2 fusion.15
  181.8 3.0 %convolution_convert_fusion = bf16[128,2048]{1,0:T(8,128)(2,1)} fusion(bf16[512,2048]{1,0:T(8,128)(2,1)} %all-gather.13.cloned.1.call-done, f32[128,512]{0,1:T(8,128)S(1)} %get-tuple-element.415, f32[512]{0:T(512)} %convert_element_type.388, f32[128]{0:T(128)S(1)} %add_rsqrt_fusion), kind=kOutput, calls=%fused_computation.22 | convolution fusion | flops 268894208 | bytes 2886144 | tf_op jit(solution)/shard_map/dot_general | solution.py:284
  184.8 23.9 %reduce-scatter.2.cloned.1.call-done = bf16[32,2048]{1,0:T(8,128)(2,1)} async-done(((bf16[128,2048]{1,0:T(8,128)(2,1)}), bf16[32,2048]{1,0:T(8,128)(2,1)}) %reduce-scatter.2.cloned.1.call-update) | async-done | bytes 131088 | tf_op jit(solution)/shard_map/reduce_scatter | solution.py:283
  208.7 1.6 fusion.71
  (167 shorter events, 12.7 us)
Async XLA Ops:
  6.5 3.0 %copy-start = (bf16[3,512,512]{2,1,0:T(8,128)(2,1)S(1)}, bf16[3,512,512]{2,1,0:T(8,128)(2,1)}, u32[]{:S(2)}) copy-start(bf16[3,512,512]{2,1,0:T(8,128)(2,1)} %param.25) | copy-start | bytes 4718596
  6.5 32.2 %copy-start.16 = (bf16[2048]{0:T(1024)(128)(2,1)S(1)}, bf16[2048]{0:T(1024)(128)(2,1)}, u32[]{:S(2)}) copy-start(bf16[2048]{0:T(1024)(128)(2,1)} %param.26) | copy-start | bytes 12292
  6.5 32.2 %copy-start.2 = (bf16[1,32,2048]{2,1,0:T(8,128)(2,1)S(1)}, bf16[1,32,2048]{2,1,0:T(8,128)(2,1)}, u32[]{:S(2)}) copy-start(bf16[1,32,2048]{2,1,0:T(8,128)(2,1)} %param.21) | copy-start | bytes 393220
  6.5 32.5 %copy-start.6 = (bf16[2,1024,8]{1,2,0:T(8,128)(2,1)S(1)}, bf16[2,1024,8]{1,2,0:T(8,128)(2,1)}, u32[]{:S(2)}) copy-start(bf16[2,1024,8]{1,2,0:T(8,128)(2,1)} %param.31) | copy-start | bytes 98308
  6.5 36.8 %copy-start.11 = (bf16[3,512]{1,0:T(4,128)(2,1)S(1)}, bf16[3,512]{1,0:T(4,128)(2,1)}, u32[]{:S(2)}) copy-start(bf16[3,512]{1,0:T(4,128)(2,1)} %param.32) | copy-start | bytes 9220
  6.5 36.8 %copy-start.17 = (bf16[3,128]{1,0:T(4,128)(2,1)S(1)}, bf16[3,128]{1,0:T(4,128)(2,1)}, u32[]{:S(2)}) copy-start(bf16[3,128]{1,0:T(4,128)(2,1)} %param.33) | copy-start | bytes 2308
  6.6 56.5 %all-gather.9.cloned.1.call-start = ((), (), s32[]{:S(2)}) async-start(), calls=%async_computation.1 | async-start | bytes 3145728 | tf_op jit(solution)/shard_map/all_gather | solution.py:175
  7.3 60.1 %all-gather.11.cloned.1.call-start = ((), (), s32[]{:S(2)}) async-start(), calls=%async_computation.2 | async-start | bytes 3145728 | tf_op jit(solution)/shard_map/all_gather | solution.py:178
  8.0 168.4 %all-reduce.3.cloned.1.call-start = ((), (), s32[]{:S(2)}) async-start(), calls=%async_computation.5 | async-start | bytes 1048576 | tf_op jit(solution)/shard_map/psum | solution.py:222
  8.8 54.2 %copy-start.20 = (f32[2,8]{1,0:T(2,128)S(1)}, f32[2,8]{1,0:T(2,128)}, u32[]{:S(2)}) copy-start(f32[2,8]{1,0:T(2,128)} %param.35) | copy-start | bytes 196
  66.6 0.8 copy-start.1
  77.5 14.1 %copy-start.5 = (bf16[1,640]{0,1:T(8,128)(2,1)S(1)}, bf16[1,640]{0,1:T(8,128)(2,1)}, u32[]{:S(2)}) copy-start(bf16[1,640]{0,1:T(8,128)(2,1)} %get-tuple-element.422) | copy-start | bytes 3844
  77.5 18.0 %copy-start.4 = (bf16[1,640]{0,1:T(8,128)(2,1)S(1)}, bf16[1,640]{0,1:T(8,128)(2,1)}, u32[]{:S(2)}) copy-start(bf16[1,640]{0,1:T(8,128)(2,1)} %get-tuple-element.423) | copy-start | bytes 3844
  77.5 19.4 %copy-start.24 = (pred[4]{0:T(512)(128)(4,1)S(1)}, pred[4]{0:T(512)(128)(4,1)}, u32[]{:S(2)}) copy-start(pred[4]{0:T(512)(128)(4,1)} %get-tuple-element.456) | copy-start | bytes 16
  77.6 25.3 %slice-start = ((bf16[128,656]{0,1:T(8,128)(2,1)}), bf16[128,640]{0,1:T(8,128)(2,1)S(1)}, s32[]{:S(2)}) async-start(bf16[128,656]{0,1:T(8,128)(2,1)} %copy-done.1), calls=%async_computation.6 | async-start | bytes 327680 | tf_op jit(solution)/shard_map/slice | solution.py:200
  91.7 6.7 %collective-permute-start.2 = (bf16[1,640]{0,1:T(8,128)(2,1)S(1)}, bf16[1,640]{0,1:T(8,128)(2,1)S(1)}, u32[]{:S(2)}, u32[]{:S(2)}) collective-permute-start(bf16[1,640]{0,1:T(8,128)(2,1)S(1)} %copy-done.5), channel_id=1, source_target_pairs={{0,8},{8,16},{16,24},{1,9},{9,17},{17,25},{2,10},{10,18},{18,26},{... | collective-permute-start | bytes 3848 | tf_op jit(solution)/shard_map/ppermute | solution.py:20
  95.6 7.2 %collective-permute-start.3 = (bf16[1,640]{0,1:T(8,128)(2,1)S(1)}, bf16[1,640]{0,1:T(8,128)(2,1)S(1)}, u32[]{:S(2)}, u32[]{:S(2)}) collective-permute-start(bf16[1,640]{0,1:T(8,128)(2,1)S(1)} %copy-done.4), channel_id=1, source_target_pairs={{8,0},{16,8},{24,16},{9,1},{17,9},{25,17},{10,2},{18,10},{26,18},{... | collective-permute-start | bytes 3848 | tf_op jit(solution)/shard_map/ppermute | solution.py:21
  97.1 10.3 %copy-start.18 = (bf16[3,128]{1,0:T(4,128)(2,1)S(1)}, bf16[3,128]{1,0:T(4,128)(2,1)}, u32[]{:S(2)}) copy-start(bf16[3,128]{1,0:T(4,128)(2,1)} %param.34) | copy-start | bytes 2308
  97.1 10.9 %copy-start.19 = (bf16[512]{0:T(512)(128)(2,1)S(1)}, bf16[512]{0:T(512)(128)(2,1)}, u32[]{:S(2)}) copy-start(bf16[512]{0:T(512)(128)(2,1)} %param.36) | copy-start | bytes 3076
  106.2 75.6 %all-gather.13.cloned.1.call-start = ((), (), s32[]{:S(2)}) async-start(), calls=%async_computation.3 | async-start | bytes 3145728 | tf_op jit(solution)/shard_map/all_gather | solution.py:181
  106.7 102.0 %reduce-scatter.2.cloned.1.call-start = ((), (), s32[]{:S(2)}) async-start(), calls=%async_computation.4 | async-start | bytes 655360 | tf_op jit(solution)/shard_map/reduce_scatter | solution.py:283
  111.0 27.5 %collective-permute-start = (bf16[1,768]{0,1:T(8,128)(2,1)S(1)}, bf16[1,768]{0,1:T(8,128)(2,1)S(1)}, u32[]{:S(2)}, u32[]{:S(2)}) collective-permute-start(bf16[1,768]{0,1:T(8,128)(2,1)S(1)} %get-tuple-element.416), channel_id=1, source_target_pairs={{0,8},{8,16},{16,24},{1,9},{9,17},{17,25},{2,10},{10,18},{18,26},{... | collective-permute-start | bytes 4616 | tf_op jit(solution)/shard_map/ppermute | solution.py:20
  113.0 25.5 %collective-permute-start.1 = (bf16[1,768]{0,1:T(8,128)(2,1)S(1)}, bf16[1,768]{0,1:T(8,128)(2,1)S(1)}, u32[]{:S(2)}, u32[]{:S(2)}) collective-permute-start(bf16[1,768]{0,1:T(8,128)(2,1)S(1)} %get-tuple-element.417), channel_id=1, source_target_pairs={{8,0},{16,8},{24,16},{9,1},{17,9},{25,17},{10,2},{18,10},{26,18},{... | collective-permute-start | bytes 4616 | tf_op jit(solution)/shard_map/ppermute | solution.py:21
  137.8 3.0 %copy-start.9 = (f32[128,8]{0,1:T(8,128)S(1)}, f32[128,8]{0,1:T(8,128)}, u32[]{:S(2)}) copy-start(f32[128,8]{0,1:T(8,128)} %get-tuple-element.446) | copy-start | bytes 12292
  137.8 3.0 %copy-start.10 = (f32[128,8]{0,1:T(8,128)S(1)}, f32[128,8]{0,1:T(8,128)}, u32[]{:S(2)}) copy-start(f32[128,8]{0,1:T(8,128)} %get-tuple-element.439) | copy-start | bytes 12292
  137.8 3.1 %copy-start.23 = (f32[8]{0:T(128)S(1)}, f32[8]{0:T(128)}, u32[]{:S(2)}) copy-start(f32[8]{0:T(128)} %exponential_multiply_fusion.1) | copy-start | bytes 100
  138.8 17.4 %copy-start.13 = (f32[1,8]{1,0:T(1,128)S(1)}, f32[1,8]{1,0:T(1,128)}, u32[]{:S(2)}) copy-start(f32[1,8]{1,0:T(1,128)} %custom-call) | copy-start | bytes 100
  138.8 17.4 %copy-start.15 = (bf16[4,1,8]{2,1,0:T(2,128)(2,1)S(1)}, bf16[4,1,8]{2,1,0:T(2,128)(2,1)}, u32[]{:S(2)}) copy-start(bf16[4,1,8]{2,1,0:T(2,128)(2,1)} %all_gather.58) | copy-start | bytes 196
  140.1 17.9 %copy-start.8 = (f32[128,8]{0,1:T(8,128)S(1)}, f32[128,8]{0,1:T(8,128)}, u32[]{:S(2)}) copy-start(f32[128,8]{0,1:T(8,128)} %get-tuple-element.448) | copy-start | bytes 12292
  140.1 18.0 %copy-start.22 = (f32[8]{0:T(128)S(1)}, f32[8]{0:T(128)}, u32[]{:S(2)}) copy-start(f32[8]{0:T(128)} %exponential_multiply_fusion) | copy-start | bytes 100
  140.8 33.2 %copy-start.12 = (f32[1,8]{1,0:T(1,128)S(1)}, f32[1,8]{1,0:T(1,128)}, u32[]{:S(2)}) copy-start(f32[1,8]{1,0:T(1,128)} %custom-call.2) | copy-start | bytes 100
  140.8 33.2 %copy-start.14 = (bf16[4,1,8]{2,1,0:T(2,128)(2,1)S(1)}, bf16[4,1,8]{2,1,0:T(2,128)(2,1)}, u32[]{:S(2)}) copy-start(bf16[4,1,8]{2,1,0:T(2,128)(2,1)} %all_gather.62) | copy-start | bytes 196
  156.8 19.6 %copy-start.7 = (f32[128,8]{0,1:T(8,128)S(1)}, f32[128,8]{0,1:T(8,128)}, u32[]{:S(2)}) copy-start(f32[128,8]{0,1:T(8,128)} %get-tuple-element.447) | copy-start | bytes 12292
  156.8 19.6 %copy-start.21 = (f32[8]{0:T(128)S(1)}, f32[8]{0:T(128)}, u32[]{:S(2)}) copy-start(f32[8]{0:T(128)} %get-tuple-element.426) | copy-start | bytes 100
  174.8 5.7 %copy-start.3 = (f32[128,512]{0,1:T(8,128)S(1)}, f32[128,512]{0,1:T(8,128)}, u32[]{:S(2)}) copy-start(f32[128,512]{0,1:T(8,128)} %get-tuple-element.418) | copy-start | bytes 786436
Sparse Core Ops, SparseCore 0:
  8.9 13.3 all-gather.8
  23.8 11.7 all-gather.10
  106.3 40.7 all-reduce.2
  148.5 10.0 all-gather.12
  184.9 23.7 reduce-scatter.1
where the time goes:
time: 218 us; the launch traced here: 217 us
  blocking collectives  110 us (50%)
  waiting for transfers between devices  31.4 us (14%)
  matrix products  20.7 us (9%)
  other arithmetic  16.4 us (8%)
  local copies, waits for them, and re-layouts  15.9 us (7%)
  between operations  13.8 us (6%)
  starting transfers between devices  8.63 us (4%)
    all_gather x4, blocking collectives, carried_in_2(): lax.all_gather(part.astype(kind), axis)  51.8 us
    reduce_scatter x1, waiting for transfers between devices, shards(): lax.psum_scatter(jnp.dot(normed_out, full_out, preferred_element_type=jnp...  23.9 us
    psum x1, blocking collectives, shards(): summed = lax.psum(partial_value, 'sp')  20.4 us
    concatenate x1, local copies, waits for them, and re-layouts, shards(): jnp.concatenate([full_x, full_b, full_c, full_fwd, full_bwd, full_z], axi...  10.2 us
    all_gather x1, blocking collectives, shards(): lax.all_gather(latent_rows, 'tp', axis=0, tiled=True)  10 us
    all_gather x1, blocking collectives, shards(): mod_vectors = lax.all_gather(summed, 'tp', axis=2, tiled=True)  8.34 us
    all_gather x1, blocking collectives, shards(): lax.all_gather(jnp.stack([total_fwd, total_bwd])[None], 'sp', axis=0, til...  7.58 us
    ppermute x2, starting transfers between devices, with_halo(): before = lax.ppermute(last, axis, up)  5.86 us
  transfers between devices with their start and end apart: 9, of which 3 were waited for; matrix products, arithmetic and copies ran while one was open for 13% of the time, Pallas kernels for 0%

commit v1 on v0

v1 whole, which is shorter than its diff:
```python
import functools

import jax
import jax.numpy as jnp
from jax import lax
from jax.experimental import pallas as pl
from jax.experimental.pallas import tpu as pltpu
from jax.sharding import PartitionSpec as P

STATE = 128
LANES = 128
PAD = 16
EPSILON = 1e-06
MESH = pl.DeviceIdType.MESH
F32 = jnp.float32
BF16 = jnp.bfloat16


def silu(v):
    return v / (1.0 + jnp.exp(-v))


def softplus(v):
    return jnp.maximum(v, 0.0) + jnp.log1p(jnp.exp(-jnp.abs(v)))


def dot(a, b, dims=((1,), (0,)), precision=None):
    return lax.dot_general(a, b, (dims, ((), ())), precision=precision, preferred_element_type=F32)


def kernel(
    n_sp,
    n_tp,
    n_dp,
    heads,
    acts,
    edges,
    gain,
    conv_x,
    conv_b,
    conv_c,
    rate,
    out_gain,
    latent,
    context,
    mod_weight,
    w_x,
    w_b,
    w_c,
    w_dt,
    w_z,
    w_out,
    out,
    lat_all,
    ctx_buf,
    mod_buf,
    wx,
    wb,
    wc,
    wd,
    wz,
    wo,
    part,
    part_all,
    mods,
    halo,
    hid,
    snd_a,
    rcv_a,
    tot,
    snd_b,
    rcv_b,
    snd_o,
    rcv_o,
    local_sem,
    dp_send,
    dp_recv,
    lat_send,
    lat_recv,
    mod1_send,
    mod1_recv,
    mod2_send,
    mod2_recv,
    edge_send,
    edge_recv,
    a_send,
    a_recv,
    t_send,
    t_recv,
    b_send,
    b_recv,
    o_send,
    o_recv,
):
    s = lax.axis_index("sp")
    t = lax.axis_index("tp")
    d = lax.axis_index("dp")
    own_rows, width = latent.shape
    ctx_rows = context.shape[0]
    rows = n_tp * own_rows
    inner = w_x.shape[1]
    both = 2 * inner
    head_dim = inner // heads
    nh2 = 2 * heads

    def remote(src, dst, send, recv, **to):
        return pltpu.make_async_remote_copy(
            src_ref=src, dst_ref=dst, send_sem=send, recv_sem=recv, device_id=to, device_id_type=MESH
        )

    local = []

    def fetch(src, dst):
        copy = pltpu.make_async_copy(src, dst, local_sem.at[len(local)])
        copy.start()
        local.append(copy)
        return copy

    mod_copy = fetch(mod_weight, mod_buf)
    lat_copy = fetch(latent, lat_all.at[t])
    ctx_copy = fetch(context, ctx_buf)
    lat_moves = []
    for k in range(1, n_tp):
        lat_moves.append(
            remote(latent, lat_all.at[t], lat_send.at[k], lat_recv.at[k], tp=lax.rem(t + k, n_tp))
        )
        lat_moves[-1].start()
    up, down = lax.rem(s + 1, n_sp), lax.rem(s + n_sp - 1, n_sp)
    ctx_up = remote(edges.at[3], halo.at[2], edge_send.at[0], edge_recv.at[2], sp=up)
    ctx_down = remote(edges.at[2], halo.at[3], edge_send.at[1], edge_recv.at[3], sp=down)
    ctx_up.start()
    ctx_down.start()
    lat_up = [
        remote(edges.at[1], halo.at[0], edge_send.at[2 + u], edge_recv.at[0], sp=up, tp=u)
        for u in range(n_tp)
    ]
    lat_down = [
        remote(edges.at[0], halo.at[1], edge_send.at[2 + n_tp + u], edge_recv.at[1], sp=down, tp=u)
        for u in range(n_tp)
    ]

    @pl.when(t == n_tp - 1)
    def _():
        for copy in lat_up:
            copy.start()

    @pl.when(t == 0)
    def _():
        for copy in lat_down:
            copy.start()

    weight_moves = []
    pairs = ((w_x, wx), (w_b, wb), (w_dt, wd), (w_c, wc), (w_z, wz), (w_out, wo))
    for i, (src, dst) in enumerate(pairs):
        depth = src.shape[0]
        place = dst.at[pl.ds(d * depth, depth)]
        for k in range(1, n_dp):
            at = i * n_dp + k
            weight_moves.append(
                remote(src, place, dp_send.at[at], dp_recv.at[at], dp=lax.rem(d + k, n_dp))
            )
            weight_moves[-1].start()
        fetch(src, place)

    mod_copy.wait()
    pieces = [dot(acts[...], mod_buf[k])[0:2] for k in range(mod_buf.shape[0])]
    cols = pieces[0].shape[1]
    part[...] = jnp.concatenate(pieces + [jnp.zeros((2, cols), F32)], axis=0)
    moves = []
    for k in range(1, n_sp):
        moves.append(
            remote(part, part_all.at[k], mod1_send.at[k], mod1_recv.at[k], sp=lax.rem(s + k, n_sp))
        )
        moves[-1].start()
    summed = part[...]
    for k in range(1, n_sp):
        moves[k - 1].wait()
        summed = summed + part_all[k]
    mods[t] = summed
    moves = []
    for k in range(1, n_tp):
        moves.append(
            remote(mods.at[t], mods.at[t], mod2_send.at[k], mod2_recv.at[k], tp=lax.rem(t + k, n_tp))
        )
        moves[-1].start()
    for copy in moves:
        copy.wait()

    def vector(row):
        return jnp.concatenate([mods[c][row : row + 1] for c in range(n_tp)], axis=1)

    def normed(v, gains, shift):
        return v * lax.rsqrt(jnp.mean(v * v, axis=1, keepdims=True) + EPSILON) * gains + shift

    gain_row = gain[...].astype(F32)
    lat_shift, ctx_shift = vector(0), vector(1)
    lat_gain = gain_row * (1.0 + vector(2))
    ctx_gain = gain_row * (1.0 + vector(3))
    ctx_copy.wait()
    step_rows = min(32, ctx_rows)
    for r in range(0, ctx_rows, step_rows):
        block = ctx_buf[r : r + step_rows].astype(F32)
        hid[rows + PAD + r : rows + PAD + r + step_rows] = normed(block, ctx_gain, ctx_shift).astype(BF16)
    lat_copy.wait()
    for copy in lat_moves:
        copy.wait()
    for u in range(n_tp):
        hid[u * own_rows : (u + 1) * own_rows] = normed(
            lat_all[u].astype(F32), lat_gain, lat_shift
        ).astype(BF16)
    ctx_up.wait_send()
    ctx_down.wait_send()
    ctx_up.wait_recv()
    ctx_down.wait_recv()
    lat_up[0].wait_recv()
    lat_down[0].wait_recv()

    @pl.when(t == n_tp - 1)
    def _():
        for copy in lat_up:
            copy.wait_send()

    @pl.when(t == 0)
    def _():
        for copy in lat_down:
            copy.wait_send()

    hid[rows : rows + PAD] = jnp.concatenate(
        [
            normed(halo[0], lat_gain, lat_shift),
            normed(halo[1], lat_gain, lat_shift),
            normed(halo[2], ctx_gain, ctx_shift),
            normed(halo[3], ctx_gain, ctx_shift),
            jnp.zeros((PAD - 4, width), F32),
        ],
        axis=0,
    ).astype(BF16)
    for copy in weight_moves:
        copy.wait()
    for copy in local[3:]:
        copy.wait()

    has_before = s > 0
    has_after = s < n_sp - 1

    def shaped(values, before, after, taps):
        count = values.shape[0]
        at = lax.broadcasted_iota(jnp.int32, values.shape, 0)
        before = jnp.where(has_before, before, 0.0)
        after = jnp.where(has_after, after, 0.0)
        earlier = jnp.where(at == 0, before, pltpu.roll(values, 1, 0))
        later = jnp.where(at == count - 1, after, pltpu.roll(values, count - 1, 0))
        w = taps[...].astype(F32)
        return silu(earlier * w[0:1] + values * w[1:2] + later * w[2:3]).astype(BF16)

    def project(weight, count):
        return dot(hid[0:count], weight[...]).astype(BF16).astype(F32)

    total = rows + PAD + ctx_rows
    px = project(wx, total)
    x_in = shaped(px[0:rows], px[rows : rows + 1], px[rows + 1 : rows + 2], conv_x).astype(F32)
    cx_in = shaped(
        px[rows + PAD :], px[rows + 2 : rows + 3], px[rows + 3 : rows + 4], conv_x
    ).astype(F32)
    pb = project(wb, total)
    b_in = shaped(pb[0:rows], pb[rows : rows + 1], pb[rows + 1 : rows + 2], conv_b)
    cb_in = shaped(pb[rows + PAD :], pb[rows + 2 : rows + 3], pb[rows + 3 : rows + 4], conv_b)
    step_all = softplus(project(wd, total))

    spread_at = lax.broadcasted_iota(jnp.int32, (LANES, both), 0)
    spread_to = lax.broadcasted_iota(jnp.int32, (LANES, both), 1) // head_dim
    spreader = jnp.where((spread_to == spread_at) | (spread_to + nh2 == spread_at), 1.0, 0.0).astype(BF16)

    def expand(v):
        lane = lax.broadcasted_iota(jnp.int32, v.shape, 1)
        high = v.astype(BF16).astype(F32)
        low = pltpu.roll(v - high, nh2, 1)
        packed = jnp.where(lane < nh2, high, jnp.where(lane < 2 * nh2, low, 0.0))
        return dot(packed.astype(BF16), spreader)

    def running(steps):
        count = steps.shape[0]
        logs = -rate[...] * steps
        a = lax.broadcasted_iota(jnp.int32, (count, count), 0)
        b = lax.broadcasted_iota(jnp.int32, (count, count), 1)
        lower = jnp.where(a >= b, 1.0, 0.0)
        upper = jnp.where(a <= b, 1.0, 0.0)
        lane = lax.broadcasted_iota(jnp.int32, logs.shape, 1)
        sums = jnp.where(
            lane < heads,
            dot(lower, logs, precision=lax.Precision.HIGHEST),
            dot(upper, logs, precision=lax.Precision.HIGHEST),
        )
        row_lane = lax.broadcasted_iota(jnp.int32, (1, LANES), 1)
        ends = jnp.where(row_lane < heads, sums[count - 1 : count], sums[0:1])
        return sums, ends

    def moved(values, steps):
        wide = jnp.concatenate([values, values], axis=1)
        return (wide * expand(steps)).astype(BF16)

    c_steps = step_all[rows + PAD :]
    c_sums, c_ends = running(c_steps)
    c_moved = moved(cx_in, c_steps)
    c_scaled = (c_moved.astype(F32) * expand(jnp.exp(c_ends - c_sums))).astype(BF16)
    c_state = dot(cb_in, c_scaled, ((0,), (0,)))
    l_steps = step_all[0:rows]
    l_sums, l_ends = running(l_steps)
    l_moved = moved(x_in, l_steps)
    l_scaled = (l_moved.astype(F32) * expand(jnp.exp(l_ends - l_sums))).astype(BF16)
    l_state = dot(b_in, l_scaled, ((0,), (0,)))
    state_rows = STATE // n_sp
    for r in range(n_sp):
        cut = slice(r * state_rows, (r + 1) * state_rows)
        snd_a[r, :, 0:both] = c_state[cut].astype(BF16)
        snd_a[r, :, both : 2 * both] = l_state[cut].astype(BF16)
    ends = jnp.exp(jnp.concatenate([c_ends, l_ends, jnp.zeros((6, LANES), F32)], axis=0))
    tot[s] = expand(ends)
    a_moves, t_moves = [], []
    for k in range(1, n_sp):
        to = lax.rem(s + k, n_sp)
        a_moves.append(remote(snd_a.at[to], rcv_a.at[s], a_send.at[k], a_recv.at[k], sp=to))
        a_moves[-1].start()
        t_moves.append(remote(tot.at[s], tot.at[s], t_send.at[k], t_recv.at[k], sp=to))
        t_moves[-1].start()
    rcv_a[s] = snd_a[s]

    pc = project(wc, rows + PAD)
    c_in = shaped(pc[0:rows], pc[rows : rows + 1], pc[rows + 1 : rows + 2], conv_c)
    scores = dot(c_in, b_in, ((1,), (1,)))
    at_t = lax.broadcasted_iota(jnp.int32, (rows, rows), 0)
    at_s = lax.broadcasted_iota(jnp.int32, (rows, rows), 1)
    sums_t = jnp.transpose(l_sums)

    def weights(lane, keep):
        gap = l_sums[:, lane : lane + 1] - sums_t[lane : lane + 1]
        return jnp.where(keep, scores * jnp.exp(jnp.minimum(gap, 0.0)), 0.0).astype(BF16)

    pair = LANES // head_dim
    inside = []
    lane_head = lax.broadcasted_iota(jnp.int32, (rows, LANES), 1) // head_dim
    for p in range(heads // pair):
        cut = slice(p * LANES, (p + 1) * LANES)
        cut_b = slice(inner + p * LANES, inner + (p + 1) * LANES)
        source = jnp.concatenate([l_moved[:, cut], l_moved[:, cut_b]], axis=0)
        value = None
        for i in range(pair):
            h = p * pair + i
            w = jnp.concatenate([weights(h, at_t >= at_s), weights(heads + h, at_t <= at_s)], axis=1)
            one = dot(w, source)
            value = one if value is None else jnp.where(lane_head == i, one, value)
        inside.append(value)
    inside = jnp.concatenate(inside, axis=1)
    growth = expand(jnp.exp(l_sums))
    gate = silu(project(wz, rows))

    for copy in a_moves + t_moves:
        copy.wait()
    entering = None
    ctx_f = ctx_b = None
    for j in range(n_sp):
        mine = rcv_a[j, :, 0:inner].astype(F32)
        ctx_f = mine if ctx_f is None else ctx_f * tot[j, 0:1, 0:inner] + mine
        i = n_sp - 1 - j
        mine = rcv_a[i, :, inner:both].astype(F32)
        ctx_b = mine if ctx_b is None else ctx_b * tot[i, 0:1, inner:both] + mine
    for j in range(n_sp):
        snd_b[j, :, 0:inner] = ctx_f.astype(BF16)
        ctx_f = ctx_f * tot[j, 1:2, 0:inner] + rcv_a[j, :, both : both + inner].astype(F32)
        i = n_sp - 1 - j
        snd_b[i, :, inner:both] = ctx_b.astype(BF16)
        ctx_b = ctx_b * tot[i, 1:2, inner:both] + rcv_a[i, :, both + inner : 2 * both].astype(F32)
    b_moves = []
    for k in range(1, n_sp):
        to = lax.rem(s + k, n_sp)
        b_moves.append(remote(snd_b.at[to], rcv_b.at[s], b_send.at[k], b_recv.at[k], sp=to))
        b_moves[-1].start()
    rcv_b[s] = snd_b[s]
    for copy in b_moves:
        copy.wait()
    entering = jnp.concatenate([rcv_b[r] for r in range(n_sp)], axis=0)
    carried = dot(c_in, entering) * growth
    gated = (inside + carried[:, 0:inner] + carried[:, inner:both]) * gate
    ny = (
        gated
        * lax.rsqrt(jnp.mean(gated * gated, axis=1, keepdims=True) + EPSILON)
        * out_gain[...].astype(F32)
    ).astype(BF16)

    chunks = n_tp
    chunk = width // chunks
    o_moves = []
    for c in range(chunks):
        cut = slice(c * chunk, (c + 1) * chunk)
        result = dot(ny, wo[:, cut]).astype(BF16)
        for u in range(n_tp):
            snd_o[c, u] = result[u * own_rows : (u + 1) * own_rows]
        for k in range(1, n_tp):
            to = lax.rem(t + k, n_tp)
            at = c * n_tp + k
            o_moves.append(remote(snd_o.at[c, to], rcv_o.at[c, k], o_send.at[at], o_recv.at[at], tp=to))
            o_moves[-1].start()
    for c in range(chunks):
        mixed = snd_o[c, t].astype(F32)
        for k in range(1, n_tp):
            o_moves[c * (n_tp - 1) + k - 1].wait()
            mixed = mixed + rcv_o[c, k].astype(F32)
        out[:, c * chunk : (c + 1) * chunk] = (mods[c][4:5] * mixed).astype(BF16)


def shards(
    latent,
    condition,
    context,
    context_source,
    mod_weight,
    norm_gain,
    w_x,
    w_b,
    w_c,
    w_z,
    w_dt,
    conv_x,
    conv_b,
    conv_c,
    decay_rate,
    out_gain,
    w_out,
):
    n_sp, n_tp, n_dp = lax.axis_size("sp"), lax.axis_size("tp"), lax.axis_size("dp")
    own_rows, width = latent.shape[1:]
    ctx_rows = context.shape[1]
    depth = mod_weight.shape[1]
    cols = mod_weight.shape[2]
    inner = w_x.shape[1]
    heads = decay_rate.shape[1]
    both = 2 * inner
    rows = n_tp * own_rows
    state_rows = STATE // n_sp
    chunk = width // n_tp
    acts = jnp.stack([condition[0], context_source])
    acts = lax.dynamic_slice_in_dim(acts, lax.axis_index("sp") * depth, depth, 1)
    acts = jnp.pad(jax.nn.silu(acts.astype(F32)).astype(BF16), ((0, PAD - 2), (0, 0)))
    edges = jnp.stack([latent[0, 0], latent[0, -1], context[0, 0], context[0, -1]])
    edges = edges.astype(F32)[:, None, :]
    dt = jnp.concatenate([w_dt[0], w_dt[1]], axis=1)
    dt = jnp.pad(dt, ((0, 0), (0, LANES - 2 * heads)))
    rate = jnp.pad(decay_rate.reshape(1, 2 * heads), ((0, 0), (0, LANES - 2 * heads)))
    vmem = pl.BlockSpec(memory_space=pltpu.VMEM)
    anywhere = pl.BlockSpec(memory_space=pl.ANY)
    dma = pltpu.SemaphoreType.DMA
    scratch = [
        pltpu.VMEM((n_tp, own_rows, width), BF16),
        pltpu.VMEM((ctx_rows, width), BF16),
        pltpu.VMEM(mod_weight.shape, BF16),
        pltpu.VMEM((w_x.shape[0] * n_dp, inner), BF16),
        pltpu.VMEM((w_b.shape[0] * n_dp, w_b.shape[1]), BF16),
        pltpu.VMEM((w_c.shape[0] * n_dp, w_c.shape[1]), BF16),
        pltpu.VMEM((dt.shape[0] * n_dp, LANES), BF16),
        pltpu.VMEM((w_z.shape[0] * n_dp, inner), BF16),
        pltpu.VMEM((w_out.shape[0] * n_dp, width), BF16),
        pltpu.VMEM((8, cols), F32),
        pltpu.VMEM((n_sp, 8, cols), F32),
        pltpu.VMEM((n_tp, 8, cols), F32),
        pltpu.VMEM((4, 1, width), F32),
        pltpu.VMEM((rows + PAD + ctx_rows, width), BF16),
        pltpu.VMEM((n_sp, state_rows, 2 * both), BF16),
        pltpu.VMEM((n_sp, state_rows, 2 * both), BF16),
        pltpu.VMEM((n_sp, 8, both), F32),
        pltpu.VMEM((n_sp, state_rows, both), BF16),
        pltpu.VMEM((n_sp, state_rows, both), BF16),
        pltpu.VMEM((n_tp, n_tp, own_rows, chunk), BF16),
        pltpu.VMEM((n_tp, n_tp, own_rows, chunk), BF16),
        dma((9,)),
        dma((6 * n_dp,)),
        dma((6 * n_dp,)),
        dma((n_tp,)),
        dma((n_tp,)),
        dma((n_sp,)),
        dma((n_sp,)),
        dma((n_tp,)),
        dma((n_tp,)),
        dma((2 + 2 * n_tp,)),
        dma((4,)),
        dma((n_sp,)),
        dma((n_sp,)),
        dma((n_sp,)),
        dma((n_sp,)),
        dma((n_sp,)),
        dma((n_sp,)),
        dma((n_tp * n_tp,)),
        dma((n_tp * n_tp,)),
    ]
    result = pl.pallas_call(
        functools.partial(kernel, n_sp, n_tp, n_dp, heads),
        out_shape=jax.ShapeDtypeStruct((own_rows, width), BF16),
        in_specs=[vmem] * 8 + [anywhere] * 9,
        out_specs=vmem,
        scratch_shapes=scratch,
        compiler_params=pltpu.CompilerParams(
            has_side_effects=True, vmem_limit_bytes=62_000_000
        ),
    )(
        acts,
        edges,
        norm_gain[None],
        conv_x,
        conv_b,
        conv_c,
        rate,
        out_gain[None],
        latent[0],
        context[0],
        mod_weight,
        w_x,
        w_b,
        w_c,
        dt,
        w_z,
        w_out,
    )
    return result[None]


def solution(mesh):
    placed = (
        P("dp", ("sp", "tp"), None),
        P("dp", None),
        P("dp", "sp", None),
        P(),
        P(None, "sp", "tp"),
        P(),
        P("dp", "tp"),
        P("dp", "tp"),
        P("dp", "tp"),
        P("dp", "tp"),
        P(None, "dp", "tp"),
        P(None, "tp"),
        P(None, "tp"),
        P(None, "tp"),
        P(None, "tp"),
        P("tp"),
        P(("tp", "dp"), None),
    )
    return jax.shard_map(
        shards, mesh=mesh, in_specs=placed, out_specs=P("dp", ("sp", "tp"), None), check_vma=False
    )
```

time: 218 us -> 62.5 us (0.29)
  blocking collectives: 110 us -> 0 us
  Pallas kernels: 0 us -> 51.3 us
  waiting for transfers between devices: 31.4 us -> 0 us
  matrix products: 20.7 us -> 0 us
  other arithmetic: 16.4 us -> 1.44 us
  between operations: 13.8 us -> 0.03 us
  starting transfers between devices: 8.63 us -> 0 us
  local copies, waits for them, and re-layouts: 15.9 us -> 9.26 us
    all_gather x11 -> x0, blocking collectives: 89.3 us -> none  [the longest x4 51.8 us: carried_in_2(): lax.all_gather(part.astype(kind), axis)]
    pallas_call x0 -> x1, Pallas kernels: none -> 51.3 us  [shards(): pl.pallas_call(functools.partial(kernel, n_sp, n_tp, n_dp, heads), out_sh...]
    reduce_scatter x1 -> x0, waiting for transfers between devices: 23.9 us -> none  [shards(): lax.psum_scatter(jnp.dot(normed_out, full_out, preferred_element_type=jnp...]
    dot_general x14 -> x0, matrix products: 20.7 us -> none  [the longest x1 5 us: shards(): jnp.dot(lax.all_gather(latent_rows, 'tp', axis=0, tiled=True), all_weight...]
    psum x1 -> x0, blocking collectives: 20.4 us -> none  [shards(): summed = lax.psum(partial_value, 'sp')]
    concatenate x1, local copies, waits for them, and re-layouts: 10.2 us -> 0.17 us  [shards(): dt = jnp.concatenate([w_dt[0], w_dt[1]], axis=1)]
    ppermute x4 -> x0, starting transfers between devices: 8.44 us -> none  [the longest x2 5.86 us: with_halo(): before = lax.ppermute(last, axis, up)]
    ppermute x4 -> x0, waiting for transfers between devices: 5.57 us -> none  [the longest x2 4.41 us: with_halo(): after = lax.ppermute(leading, axis, down)]
  transfers between devices with their start and end apart: 9 -> 0, of which waited for: 3 -> 0; matrix products, arithmetic and copies ran while one was open for 13% -> 0% of each run, Pallas kernels for 0% -> 0%
where the time goes in v1:
time: 62.5 us; the launch traced here: 62 us
  Pallas kernels  51.3 us (82%)
  local copies, waits for them, and re-layouts  9.26 us (15%)
  other arithmetic  1.44 us (2%)
    pallas_call x1, Pallas kernels, shards(): pl.pallas_call(functools.partial(kernel, n_sp, n_tp, n_dp, heads), out_sh...  51.3 us
    unnamed x1, local copies, waits for them, and re-layouts  1.57 us
    broadcast_in_dim x1, local copies, waits for them, and re-layouts, shards(): norm_gain[None]  1.29 us
    broadcast_in_dim x1, local copies, waits for them, and re-layouts, shards(): out_gain[None]  1.26 us

profile of v1, /device:TPU:0, one launch (start us, length us, event | category | flops | bytes accessed | tf_op | source)
XLA Modules:
  0.0 62.0 jit_solution(8204284111117701461)
XLA Ops:
  0.0 0.8 %fusion.4 = (bf16[1,1,2048]{2,1,0:T(2,128)(2,1)S(1)}, bf16[1,1,2048]{2,1,0:T(2,128)(2,1)S(1)}, bf16[1,1,2048]{2,1,0:T(2,128)(2,1)S(1)}, bf16[1,1,2048]{2,1,0:T(2,128)(2,1)S(1)}) fusion(bf16[1,128,2048]{2,1,0:T(8,128)(2,1)} %param.19, bf16[1,32,2048]{2,1,0:T(8,128)(2,1)} %param.17), kind=kLoop, calls=%fused_computation.12 | loop fusion | bytes 32768 | tf_op jit(solution)/shard_map/slice | solution.py:444
  0.8 0.7 %maximum_convert_fusion.edges = f32[4,1,2048]{2,1,0:T(1,128)} fusion(bf16[1,1,2048]{2,1,0:T(2,128)(2,1)S(1)} %get-tuple-element.6, bf16[1,1,2048]{2,1,0:T(2,128)(2,1)S(1)} %get-tuple-element.5, bf16[1,1,2048]{2,1,0:T(2,128)(2,1)S(1)} %get-tuple-element.11, bf16[1,1,2048]{2,1,0:T(2,128)(2,1)S(1)} %get-tuple-element.12), kind=kLoop, calls=%fused_computation | loop fusion | flops 32768 | bytes 49152 | tf_op jit(solution)/shard_map/convert_element_type | solution.py:445
  1.5 0.7 %stack.9 = bf16[1,2048]{1,0:T(2,128)(2,1)S(1)} reshape(bf16[2048]{0:T(1024)(128)(2,1)} %param.20) | data formatting | bytes 8192 | tf_op jit(solution)/shard_map/stack | solution.py:441
  2.2 0.8 %fusion.2 = bf16[2,512]{1,0:T(2,128)(2,1)S(1)} fusion(s32[]{:T(128)S(6)} %select_n.3, bf16[1,2048]{1,0:T(2,128)(2,1)S(1)} %stack.9, bf16[1,2048]{1,0:T(2,128)(2,1)} %param.18), kind=kLoop, calls=%fused_computation.10 | loop fusion | flops 9216 | bytes 10244 | tf_op jit(solution)/shard_map/convert_element_type | solution.py:443
  3.0 0.6 pad.12.acts
  3.6 0.7 %slice_bitcast_fusion.1 = (bf16[1024,8]{0,1:T(8,128)(2,1)S(1)}, bf16[1024,8]{0,1:T(8,128)(2,1)S(1)}) fusion(bf16[2,1024,8]{1,2,0:T(8,128)(2,1)} %param.27), kind=kLoop, calls=%fused_computation.3 | loop fusion | bytes 65536 | tf_op jit(solution)/shard_map/squeeze | solution.py:446
  4.3 0.2 copy.20
  4.5 0.7 %pad.14.w_dt = bf16[1024,128]{1,0:T(8,128)(2,1)} pad(bf16[1024,16]{1,0:T(8,128)(2,1)S(1)} %copy.20, bf16[]{:T(256)} %constant.16.clone.1), padding=0_0x0_112 | pad | bytes 294914 | tf_op jit(solution)/shard_map/jit(_pad)/pad | solution.py:447
  5.3 1.3 %broadcast_in_dim.10.gain = bf16[1,2048]{1,0:T(2,128)(2,1)} reshape(bf16[2048]{0:T(1024)(128)(2,1)} %param.22) | data formatting | bytes 8192 | tf_op jit(solution)/shard_map/broadcast_in_dim | solution.py:506
  6.5 1.3 %broadcast_in_dim.11.out_gain = bf16[1,512]{1,0:T(2,128)(2,1)} reshape(bf16[512]{0:T(512)(128)(2,1)} %param.32) | data formatting | bytes 2048 | tf_op jit(solution)/shard_map/broadcast_in_dim | solution.py:511
  7.8 0.8 %reshape.50 = f32[1,16]{1,0:T(1,128)S(1)} reshape(f32[2,8]{1,0:T(2,128)} %param.31) | data formatting | bytes 128 | tf_op jit(solution)/shard_map/reshape | solution.py:448
  8.6 0.6 pad.13.rate
  9.2 51.3 %shard_map.163 = bf16[32,2048]{1,0:T(8,128)(2,1)} custom-call(bf16[16,512]{1,0:T(8,128)(2,1)} %pad.12.acts, f32[4,1,2048]{2,1,0:T(1,128)} %maximum_convert_fusion.edges, bf16[1,2048]{1,0:T(2,128)(2,1)} %broadcast_in_dim.10.gain, bf16[3,512]{1,0:T(4,128)(2,1)} %conv_x.1, bf16[3,128]{1,0:T(4,128)(2,1)} %conv_b.1, bf16[3,128]{1,0:T(4,128)(2,1)} %conv_c.1, ...), custom_call_target="tpu_custom_call" | custom-call | tf_op jit(solution)/shard_map/pallas_call | solution.py:494
  60.5 1.6 %copy.22 = bf16[1,32,2048]{2,1,0:T(8,128)(2,1)} copy(bf16[1,32,2048]{2,1,0:T(8,128)(2,1)} %bitcast.8) | data formatting | bytes 262144
  (1 shorter events, 0.0 us)

commit v2 on v1

--- a/solution.py
+++ b/solution.py
@@ -24,6 +24,10 @@
     return jnp.maximum(v, 0.0) + jnp.log1p(jnp.exp(-jnp.abs(v)))
 
 
+def row_of(ref):
+    return ref[...].astype(F32).reshape(1, ref.shape[0])
+
+
 def dot(a, b, dims=((1,), (0,)), precision=None):
     return lax.dot_general(a, b, (dims, ((), ())), precision=precision, preferred_element_type=F32)
 
@@ -33,8 +37,8 @@
     n_tp,
     n_dp,
     heads,
-    acts,
-    edges,
+    condition,
+    source,
     gain,
     conv_x,
     conv_b,
@@ -60,6 +64,8 @@
     wd,
     wz,
     wo,
+    acts,
+    edges,
     part,
     part_all,
     mods,
@@ -97,6 +103,7 @@
     d = lax.axis_index("dp")
     own_rows, width = latent.shape
     ctx_rows = context.shape[0]
+    depth = mod_weight.shape[1]
     rows = n_tp * own_rows
     inner = w_x.shape[1]
     both = 2 * inner
@@ -125,6 +132,39 @@
             remote(latent, lat_all.at[t], lat_send.at[k], lat_recv.at[k], tp=lax.rem(t + k, n_tp))
         )
         lat_moves[-1].start()
+    weight_moves = []
+    pairs = ((w_x, wx), (w_b, wb), (w_dt, wd), (w_c, wc), (w_z, wz), (w_out, wo))
+    for i, (src, dst) in enumerate(pairs):
+        count = src.shape[0]
+        place = dst.at[d] if src is w_dt else dst.at[pl.ds(d * count, count)]
+        for k in range(1, n_dp):
+            at = i * n_dp + k
+            weight_moves.append(
+                remote(src, place, dp_send.at[at], dp_recv.at[at], dp=lax.rem(d + k, n_dp))
+            )
+            weight_moves[-1].start()
+        fetch(src, place)
+
+    active = silu(jnp.concatenate([condition[...].astype(F32), row_of(source)], axis=0))
+    for j in range(n_sp):
+        acts[j, 0:2] = active[:, j * depth : (j + 1) * depth]
+    own_acts = jnp.concatenate([acts[s, 0:2], jnp.zeros((PAD - 2, depth), F32)], axis=0).astype(BF16)
+    mod_copy.wait()
+    pieces = [dot(own_acts, mod_buf[k])[0:2] for k in range(mod_buf.shape[0])]
+    cols = pieces[0].shape[1]
+    part[...] = jnp.concatenate(pieces + [jnp.zeros((2, cols), F32)], axis=0)
+    moves = []
+    for k in range(1, n_sp):
+        moves.append(
+            remote(part, part_all.at[k], mod1_send.at[k], mod1_recv.at[k], sp=lax.rem(s + k, n_sp))
+        )
+        moves[-1].start()
+    lat_copy.wait()
+    edges[0] = lat_all[t, 0:1].astype(F32)
+    edges[1] = lat_all[t, own_rows - 1 : own_rows].astype(F32)
+    ctx_copy.wait()
+    edges[2] = ctx_buf[0:1].astype(F32)
+    edges[3] = ctx_buf[ctx_rows - 1 : ctx_rows].astype(F32)
     up, down = lax.rem(s + 1, n_sp), lax.rem(s + n_sp - 1, n_sp)
     ctx_up = remote(edges.at[3], halo.at[2], edge_send.at[0], edge_recv.at[2], sp=up)
     ctx_down = remote(edges.at[2], halo.at[3], edge_send.at[1], edge_recv.at[3], sp=down)
@@ -149,29 +189,6 @@
         for copy in lat_down:
             copy.start()
 
-    weight_moves = []
-    pairs = ((w_x, wx), (w_b, wb), (w_dt, wd), (w_c, wc), (w_z, wz), (w_out, wo))
-    for i, (src, dst) in enumerate(pairs):
-        depth = src.shape[0]
-        place = dst.at[pl.ds(d * depth, depth)]
-        for k in range(1, n_dp):
-            at = i * n_dp + k
-            weight_moves.append(
-                remote(src, place, dp_send.at[at], dp_recv.at[at], dp=lax.rem(d + k, n_dp))
-            )
-            weight_moves[-1].start()
-        fetch(src, place)
-
-    mod_copy.wait()
-    pieces = [dot(acts[...], mod_buf[k])[0:2] for k in range(mod_buf.shape[0])]
-    cols = pieces[0].shape[1]
-    part[...] = jnp.concatenate(pieces + [jnp.zeros((2, cols), F32)], axis=0)
-    moves = []
-    for k in range(1, n_sp):
-        moves.append(
-            remote(part, part_all.at[k], mod1_send.at[k], mod1_recv.at[k], sp=lax.rem(s + k, n_sp))
-        )
-        moves[-1].start()
     summed = part[...]
     for k in range(1, n_sp):
         moves[k - 1].wait()
@@ -192,16 +209,14 @@
     def normed(v, gains, shift):
         return v * lax.rsqrt(jnp.mean(v * v, axis=1, keepdims=True) + EPSILON) * gains + shift
 
-    gain_row = gain[...].astype(F32)
+    gain_row = row_of(gain)
     lat_shift, ctx_shift = vector(0), vector(1)
     lat_gain = gain_row * (1.0 + vector(2))
     ctx_gain = gain_row * (1.0 + vector(3))
-    ctx_copy.wait()
     step_rows = min(32, ctx_rows)
     for r in range(0, ctx_rows, step_rows):
         block = ctx_buf[r : r + step_rows].astype(F32)
         hid[rows + PAD + r : rows + PAD + r + step_rows] = normed(block, ctx_gain, ctx_shift).astype(BF16)
-    lat_copy.wait()
     for copy in lat_moves:
         copy.wait()
     for u in range(n_tp):
@@ -265,7 +280,16 @@
     pb = project(wb, total)
     b_in = shaped(pb[0:rows], pb[rows : rows + 1], pb[rows + 1 : rows + 2], conv_b)
     cb_in = shaped(pb[rows + PAD :], pb[rows + 2 : rows + 3], pb[rows + 3 : rows + 4], conv_b)
-    step_all = softplus(project(wd, total))
+    features = None
+    half = wd.shape[3]
+    for r in range(n_dp):
+        taps = jnp.concatenate(
+            [wd[r, 0].astype(F32), wd[r, 1].astype(F32), jnp.zeros((LANES - nh2, half), F32)], axis=0
+        ).astype(BF16)
+        one = dot(hid[0:total, r * half : (r + 1) * half], taps, ((1,), (1,)))
+        features = one if features is None else features + one
+    step_all = softplus(features.astype(BF16).astype(F32))
+    rates = jnp.concatenate([rate[0:1], rate[1:2], jnp.zeros((1, LANES - nh2), F32)], axis=1)
 
     spread_at = lax.broadcasted_iota(jnp.int32, (LANES, both), 0)
     spread_to = lax.broadcasted_iota(jnp.int32, (LANES, both), 1) // head_dim
@@ -280,7 +304,7 @@
 
     def running(steps):
         count = steps.shape[0]
-        logs = -rate[...] * steps
+        logs = -rates * steps
         a = lax.broadcasted_iota(jnp.int32, (count, count), 0)
         b = lax.broadcasted_iota(jnp.int32, (count, count), 1)
         lower = jnp.where(a >= b, 1.0, 0.0)
@@ -384,7 +408,7 @@
     ny = (
         gated
         * lax.rsqrt(jnp.mean(gated * gated, axis=1, keepdims=True) + EPSILON)
-        * out_gain[...].astype(F32)
+        * row_of(out_gain)
     ).astype(BF16)
 
     chunks = n_tp
@@ -438,14 +462,6 @@
     rows = n_tp * own_rows
     state_rows = STATE // n_sp
     chunk = width // n_tp
-    acts = jnp.stack([condition[0], context_source])
-    acts = lax.dynamic_slice_in_dim(acts, lax.axis_index("sp") * depth, depth, 1)
-    acts = jnp.pad(jax.nn.silu(acts.astype(F32)).astype(BF16), ((0, PAD - 2), (0, 0)))
-    edges = jnp.stack([latent[0, 0], latent[0, -1], context[0, 0], context[0, -1]])
-    edges = edges.astype(F32)[:, None, :]
-    dt = jnp.concatenate([w_dt[0], w_dt[1]], axis=1)
-    dt = jnp.pad(dt, ((0, 0), (0, LANES - 2 * heads)))
-    rate = jnp.pad(decay_rate.reshape(1, 2 * heads), ((0, 0), (0, LANES - 2 * heads)))
     vmem = pl.BlockSpec(memory_space=pltpu.VMEM)
     anywhere = pl.BlockSpec(memory_space=pl.ANY)
     dma = pltpu.SemaphoreType.DMA
@@ -456,9 +472,11 @@
         pltpu.VMEM((w_x.shape[0] * n_dp, inner), BF16),
         pltpu.VMEM((w_b.shape[0] * n_dp, w_b.shape[1]), BF16),
         pltpu.VMEM((w_c.shape[0] * n_dp, w_c.shape[1]), BF16),
-        pltpu.VMEM((dt.shape[0] * n_dp, LANES), BF16),
+        pltpu.VMEM((n_dp, 2, heads, w_dt.shape[1]), BF16),
         pltpu.VMEM((w_z.shape[0] * n_dp, inner), BF16),
         pltpu.VMEM((w_out.shape[0] * n_dp, width), BF16),
+        pltpu.VMEM((n_sp, 8, depth), F32),
+        pltpu.VMEM((4, 1, width), F32),
         pltpu.VMEM((8, cols), F32),
         pltpu.VMEM((n_sp, 8, cols), F32),
         pltpu.VMEM((n_tp, 8, cols), F32),
@@ -501,21 +519,21 @@
             has_side_effects=True, vmem_limit_bytes=62_000_000
         ),
     )(
-        acts,
-        edges,
-        norm_gain[None],
+        condition,
+        context_source,
+        norm_gain,
         conv_x,
         conv_b,
         conv_c,
-        rate,
-        out_gain[None],
+        decay_rate,
+        out_gain,
         latent[0],
         context[0],
         mod_weight,
         w_x,
         w_b,
         w_c,
-        dt,
+        jnp.swapaxes(w_dt, 1, 2),
         w_z,
         w_out,
     )

time: 62.5 us -> 53.1 us (0.85)
  local copies, waits for them, and re-layouts: 9.26 us -> 1.57 us
  other arithmetic: 1.44 us -> 0 us
    broadcast_in_dim x2 -> x0, local copies, waits for them, and re-layouts: 2.55 us -> none  [the longest x1 1.29 us: shards(): norm_gain[None]]
    pad x3 -> x0, local copies, waits for them, and re-layouts: 1.95 us -> none  [the longest x1 0.75 us: shards(): dt = jnp.pad(dt, ((0, 0), (0, LANES - 2 * heads)))]
    convert_element_type x2 -> x0, other arithmetic: 1.44 us -> none  [the longest x1 0.77 us: shards(): jax.nn.silu(acts.astype(F32)).astype(BF16)]
    slice x1 -> x0, local copies, waits for them, and re-layouts: 0.83 us -> none  [shards(): context[0, 0]]
    reshape x1 -> x0, local copies, waits for them, and re-layouts: 0.76 us -> none  [shards(): decay_rate.reshape(1, 2 * heads)]
    squeeze x1 -> x0, local copies, waits for them, and re-layouts: 0.74 us -> none  [shards(): dt = jnp.concatenate([w_dt[0], w_dt[1]], axis=1)]
    another operation x1 -> x0, local copies, waits for them, and re-layouts: 0.69 us -> none  [shards(): acts = jnp.stack([condition[0], context_source])]
where the time goes in v2:
time: 53.1 us; the launch traced here: 52.9 us
  Pallas kernels  51.3 us (97%)
  local copies, waits for them, and re-layouts  1.57 us (3%)
    pallas_call x1, Pallas kernels, shards(): pl.pallas_call(functools.partial(kernel, n_sp, n_tp, n_dp, heads), out_sh...  51.3 us
    unnamed x1, local copies, waits for them, and re-layouts  1.57 us

profile of v2, /device:TPU:0, one launch (start us, length us, event | category | flops | bytes accessed | tf_op | source)
XLA Modules:
  0.0 52.9 jit_solution(3276663189897250952)
XLA Ops:
  0.0 51.3 %shard_map.163 = bf16[32,2048]{1,0:T(8,128)(2,1)} custom-call(bf16[1,2048]{1,0:T(2,128)(2,1)} %condition.1, bf16[2048]{0:T(1024)(128)(2,1)} %source.1, bf16[2048]{0:T(1024)(128)(2,1)} %gain.1, bf16[3,512]{1,0:T(4,128)(2,1)} %conv_x.1, bf16[3,128]{1,0:T(4,128)(2,1)} %conv_b.1, bf16[3,128]{1,0:T(4,128)(2,1)} %conv_c.1, f32[2,8]{1,0:T(2,128)} %rate.1, ...), custom_call_target="tpu_custom_call" | custom-call | tf_op jit(solution)/shard_map/pallas_call | solution.py:512
  51.3 1.6 %copy.19 = bf16[1,32,2048]{2,1,0:T(8,128)(2,1)} copy(bf16[1,32,2048]{2,1,0:T(8,128)(2,1)} %bitcast.5) | data formatting | bytes 262144

commit v3 on v2

--- a/solution.py
+++ b/solution.py
@@ -71,11 +71,11 @@
     mods,
     halo,
     hid,
-    snd_a,
-    rcv_a,
+    own,
+    fade,
+    snd,
+    rcv,
     tot,
-    snd_b,
-    rcv_b,
     snd_o,
     rcv_o,
     local_sem,
@@ -89,12 +89,10 @@
     mod2_recv,
     edge_send,
     edge_recv,
-    a_send,
-    a_recv,
+    chain_send,
+    chain_recv,
     t_send,
     t_recv,
-    b_send,
-    b_recv,
     o_send,
     o_recv,
 ):
@@ -115,6 +113,22 @@
             src_ref=src, dst_ref=dst, send_sem=send, recv_sem=recv, device_id=to, device_id_type=MESH
         )
 
+    up, down = lax.rem(s + 1, n_sp), lax.rem(s + n_sp - 1, n_sp)
+    barrier = pltpu.get_barrier_semaphore()
+
+    def greet(**to):
+        pl.semaphore_signal(barrier, inc=1, device_id=to, device_id_type=MESH)
+
+    for k in range(1, n_sp):
+        greet(sp=lax.rem(s + k, n_sp))
+    for k in range(1, n_tp):
+        beside = lax.rem(t + k, n_tp)
+        greet(tp=beside)
+        greet(sp=up, tp=beside)
+        greet(sp=down, tp=beside)
+    for k in range(1, n_dp):
+        greet(dp=lax.rem(d + k, n_dp))
+
     local = []
 
     def fetch(src, dst):
@@ -131,7 +145,6 @@
         lat_moves.append(
             remote(latent, lat_all.at[t], lat_send.at[k], lat_recv.at[k], tp=lax.rem(t + k, n_tp))
         )
-        lat_moves[-1].start()
     weight_moves = []
     pairs = ((w_x, wx), (w_b, wb), (w_dt, wd), (w_c, wc), (w_z, wz), (w_out, wo))
     for i, (src, dst) in enumerate(pairs):
@@ -142,7 +155,6 @@
             weight_moves.append(
                 remote(src, place, dp_send.at[at], dp_recv.at[at], dp=lax.rem(d + k, n_dp))
             )
-            weight_moves[-1].start()
         fetch(src, place)
 
     active = silu(jnp.concatenate([condition[...].astype(F32), row_of(source)], axis=0))
@@ -153,19 +165,21 @@
     pieces = [dot(own_acts, mod_buf[k])[0:2] for k in range(mod_buf.shape[0])]
     cols = pieces[0].shape[1]
     part[...] = jnp.concatenate(pieces + [jnp.zeros((2, cols), F32)], axis=0)
+    pl.semaphore_wait(barrier, n_sp + 3 * n_tp + n_dp - 5)
     moves = []
     for k in range(1, n_sp):
         moves.append(
             remote(part, part_all.at[k], mod1_send.at[k], mod1_recv.at[k], sp=lax.rem(s + k, n_sp))
         )
         moves[-1].start()
+    for copy in lat_moves + weight_moves:
+        copy.start()
     lat_copy.wait()
     edges[0] = lat_all[t, 0:1].astype(F32)
     edges[1] = lat_all[t, own_rows - 1 : own_rows].astype(F32)
     ctx_copy.wait()
     edges[2] = ctx_buf[0:1].astype(F32)
     edges[3] = ctx_buf[ctx_rows - 1 : ctx_rows].astype(F32)
-    up, down = lax.rem(s + 1, n_sp), lax.rem(s + n_sp - 1, n_sp)
     ctx_up = remote(edges.at[3], halo.at[2], edge_send.at[0], edge_recv.at[2], sp=up)
     ctx_down = remote(edges.at[2], halo.at[3], edge_send.at[1], edge_recv.at[3], sp=down)
     ctx_up.start()
@@ -272,14 +286,6 @@
         return dot(hid[0:count], weight[...]).astype(BF16).astype(F32)
 
     total = rows + PAD + ctx_rows
-    px = project(wx, total)
-    x_in = shaped(px[0:rows], px[rows : rows + 1], px[rows + 1 : rows + 2], conv_x).astype(F32)
-    cx_in = shaped(
-        px[rows + PAD :], px[rows + 2 : rows + 3], px[rows + 3 : rows + 4], conv_x
-    ).astype(F32)
-    pb = project(wb, total)
-    b_in = shaped(pb[0:rows], pb[rows : rows + 1], pb[rows + 1 : rows + 2], conv_b)
-    cb_in = shaped(pb[rows + PAD :], pb[rows + 2 : rows + 3], pb[rows + 3 : rows + 4], conv_b)
     features = None
     half = wd.shape[3]
     for r in range(n_dp):
@@ -291,16 +297,6 @@
     step_all = softplus(features.astype(BF16).astype(F32))
     rates = jnp.concatenate([rate[0:1], rate[1:2], jnp.zeros((1, LANES - nh2), F32)], axis=1)
 
-    spread_at = lax.broadcasted_iota(jnp.int32, (LANES, both), 0)
-    spread_to = lax.broadcasted_iota(jnp.int32, (LANES, both), 1) // head_dim
-    spreader = jnp.where((spread_to == spread_at) | (spread_to + nh2 == spread_at), 1.0, 0.0).astype(BF16)
-
-    def expand(v):
-        lane = lax.broadcasted_iota(jnp.int32, v.shape, 1)
-        high = v.astype(BF16).astype(F32)
-        low = pltpu.roll(v - high, nh2, 1)
-        packed = jnp.where(lane < nh2, high, jnp.where(lane < 2 * nh2, low, 0.0))
-        return dot(packed.astype(BF16), spreader)
 
     def running(steps):
         count = steps.shape[0]
@@ -319,35 +315,112 @@
         ends = jnp.where(row_lane < heads, sums[count - 1 : count], sums[0:1])
         return sums, ends
 
+    c_steps = step_all[rows + PAD :]
+    c_sums, c_ends = running(c_steps)
+    l_steps = step_all[0:rows]
+    l_sums, l_ends = running(l_steps)
+    tot[s] = jnp.concatenate([c_ends, l_ends, jnp.zeros((6, LANES), F32)], axis=0)
+    t_moves = []
+    for k in range(1, n_sp):
+        to = lax.rem(s + k, n_sp)
+        t_moves.append(remote(tot.at[s], tot.at[s], t_send.at[k], t_recv.at[k], sp=to))
+        t_moves[-1].start()
+
+    px = project(wx, total)
+    x_in = shaped(px[0:rows], px[rows : rows + 1], px[rows + 1 : rows + 2], conv_x).astype(F32)
+    cx_in = shaped(
+        px[rows + PAD :], px[rows + 2 : rows + 3], px[rows + 3 : rows + 4], conv_x
+    ).astype(F32)
+    pb = project(wb, total)
+    b_in = shaped(pb[0:rows], pb[rows : rows + 1], pb[rows + 1 : rows + 2], conv_b)
+    cb_in = shaped(pb[rows + PAD :], pb[rows + 2 : rows + 3], pb[rows + 3 : rows + 4], conv_b)
+    spread_at = lax.broadcasted_iota(jnp.int32, (LANES, both), 0)
+    spread_to = lax.broadcasted_iota(jnp.int32, (LANES, both), 1) // head_dim
+    spreader = jnp.where((spread_to == spread_at) | (spread_to + nh2 == spread_at), 1.0, 0.0).astype(BF16)
+
+    def expand(v):
+        lane = lax.broadcasted_iota(jnp.int32, v.shape, 1)
+        high = v.astype(BF16).astype(F32)
+        low = pltpu.roll(v - high, nh2, 1)
+        packed = jnp.where(lane < nh2, high, jnp.where(lane < 2 * nh2, low, 0.0))
+        return dot(packed.astype(BF16), spreader)
+
     def moved(values, steps):
         wide = jnp.concatenate([values, values], axis=1)
         return (wide * expand(steps)).astype(BF16)
 
-    c_steps = step_all[rows + PAD :]
-    c_sums, c_ends = running(c_steps)
     c_moved = moved(cx_in, c_steps)
     c_scaled = (c_moved.astype(F32) * expand(jnp.exp(c_ends - c_sums))).astype(BF16)
     c_state = dot(cb_in, c_scaled, ((0,), (0,)))
-    l_steps = step_all[0:rows]
-    l_sums, l_ends = running(l_steps)
     l_moved = moved(x_in, l_steps)
     l_scaled = (l_moved.astype(F32) * expand(jnp.exp(l_ends - l_sums))).astype(BF16)
     l_state = dot(b_in, l_scaled, ((0,), (0,)))
-    state_rows = STATE // n_sp
-    for r in range(n_sp):
-        cut = slice(r * state_rows, (r + 1) * state_rows)
-        snd_a[r, :, 0:both] = c_state[cut].astype(BF16)
-        snd_a[r, :, both : 2 * both] = l_state[cut].astype(BF16)
-    ends = jnp.exp(jnp.concatenate([c_ends, l_ends, jnp.zeros((6, LANES), F32)], axis=0))
-    tot[s] = expand(ends)
-    a_moves, t_moves = [], []
-    for k in range(1, n_sp):
-        to = lax.rem(s + k, n_sp)
-        a_moves.append(remote(snd_a.at[to], rcv_a.at[s], a_send.at[k], a_recv.at[k], sp=to))
-        a_moves[-1].start()
-        t_moves.append(remote(tot.at[s], tot.at[s], t_send.at[k], t_recv.at[k], sp=to))
-        t_moves[-1].start()
-    rcv_a[s] = snd_a[s]
+    for copy in t_moves:
+        copy.wait()
+    row_lane = lax.broadcasted_iota(jnp.int32, (1, LANES), 1)
+    c_later = jnp.zeros((1, LANES), F32)
+    l_earlier = jnp.zeros((1, LANES), F32)
+    for j in range(n_sp):
+        left = jnp.where(row_lane < heads, 1, 0) * (s > j).astype(jnp.int32)
+        left = left + jnp.where(row_lane < heads, 0, 1) * (s < j).astype(jnp.int32)
+        right = jnp.where(row_lane < heads, 1, 0) * (s < j).astype(jnp.int32)
+        right = right + jnp.where(row_lane < heads, 0, 1) * (s > j).astype(jnp.int32)
+        c_later = c_later + jnp.where(right > 0, tot[j, 0:1], 0.0)
+        l_earlier = l_earlier + jnp.where(left > 0, tot[j, 1:2], 0.0)
+    fades = expand(
+        jnp.exp(
+            jnp.concatenate(
+                [c_later, l_earlier, l_ends, l_earlier + l_ends, jnp.zeros((4, LANES), F32)], axis=0
+            )
+        )
+    )
+    c_state = c_state * fades[0:1]
+    l_state = l_state + c_state * fades[3:4]
+    cuts = inner // LANES
+    for q in range(2):
+        for c in range(cuts):
+            at = q * inner + c * LANES
+            apart = (1 - q) * inner + c * LANES
+            own[q, 2 * c] = l_state[:, at : at + LANES]
+            own[q, 2 * c + 1] = c_state[:, apart : apart + LANES]
+            fade[q, 2 * c, 0:1] = fades[2:3, at : at + LANES]
+            fade[q, 2 * c + 1, 0:1] = jnp.ones((1, LANES), F32)
+
+    ends_chain = (s == 0) | (s == n_sp - 1)
+    near = jnp.where(2 * s < n_sp, 0, 1)
+    far = 1 - near
+    messages = 2 * cuts
+
+    def comes(q):
+        return jnp.where(q == 0, s, n_sp - 1 - s) > 0
+
+    def goes(q):
+        return jnp.where(q == 0, n_sp - 1 - s, s) > 0
+
+    def message(q, m):
+        to = jnp.where(q == 0, up, down)
+        return remote(snd.at[q, m], rcv.at[q, m], chain_send.at[q, m], chain_recv.at[q, m], sp=to)
+
+    def hop(q, m):
+        @pl.when(comes(q))
+        def _():
+            message(q, m).wait_recv()
+
+        @pl.when(goes(q))
+        def _():
+            snd[q, m] = (own[q, m] + rcv[q, m].astype(F32) * fade[q, m, 0:1]).astype(BF16)
+            message(q, m).start()
+
+    for q in range(2):
+
+        @pl.when(jnp.logical_not(comes(q)))
+        def _():
+            rcv[q] = jnp.zeros(rcv.shape[1:], BF16)
+
+    @pl.when(ends_chain)
+    def _():
+        for m in range(messages):
+            hop(near, m)
 
     pc = project(wc, rows + PAD)
     c_in = shaped(pc[0:rows], pc[rows : rows + 1], pc[rows + 1 : rows + 2], conv_c)
@@ -378,31 +451,30 @@
     growth = expand(jnp.exp(l_sums))
     gate = silu(project(wz, rows))
 
-    for copy in a_moves + t_moves:
-        copy.wait()
-    entering = None
-    ctx_f = ctx_b = None
-    for j in range(n_sp):
-        mine = rcv_a[j, :, 0:inner].astype(F32)
-        ctx_f = mine if ctx_f is None else ctx_f * tot[j, 0:1, 0:inner] + mine
-        i = n_sp - 1 - j
-        mine = rcv_a[i, :, inner:both].astype(F32)
-        ctx_b = mine if ctx_b is None else ctx_b * tot[i, 0:1, inner:both] + mine
-    for j in range(n_sp):
-        snd_b[j, :, 0:inner] = ctx_f.astype(BF16)
-        ctx_f = ctx_f * tot[j, 1:2, 0:inner] + rcv_a[j, :, both : both + inner].astype(F32)
-        i = n_sp - 1 - j
-        snd_b[i, :, inner:both] = ctx_b.astype(BF16)
-        ctx_b = ctx_b * tot[i, 1:2, inner:both] + rcv_a[i, :, both + inner : 2 * both].astype(F32)
-    b_moves = []
-    for k in range(1, n_sp):
-        to = lax.rem(s + k, n_sp)
-        b_moves.append(remote(snd_b.at[to], rcv_b.at[s], b_send.at[k], b_recv.at[k], sp=to))
-        b_moves[-1].start()
-    rcv_b[s] = snd_b[s]
-    for copy in b_moves:
-        copy.wait()
-    entering = jnp.concatenate([rcv_b[r] for r in range(n_sp)], axis=0)
+    lag = messages // 2
+
+    @pl.when(jnp.logical_not(ends_chain))
+    def _():
+        for m in range(messages + lag):
+            if m < messages:
+                hop(near, m)
+            if m >= lag:
+                hop(far, m - lag)
+
+    @pl.when(ends_chain)
+    def _():
+        for m in range(messages):
+            hop(far, m)
+
+    entering = []
+    for q in range(2):
+        for c in range(cuts):
+            at = q * inner + c * LANES
+            context_sum = own[1 - q, 2 * c + 1] + rcv[1 - q, 2 * c + 1].astype(F32)
+            entering.append(
+                (rcv[q, 2 * c].astype(F32) + context_sum * fades[1:2, at : at + LANES]).astype(BF16)
+            )
+    entering = jnp.concatenate(entering, axis=1)
     carried = dot(c_in, entering) * growth
     gated = (inside + carried[:, 0:inner] + carried[:, inner:both]) * gate
     ny = (
@@ -424,6 +496,13 @@
             at = c * n_tp + k
             o_moves.append(remote(snd_o.at[c, to], rcv_o.at[c, k], o_send.at[at], o_recv.at[at], tp=to))
             o_moves[-1].start()
+    for q in range(2):
+
+        @pl.when(goes(q))
+        def _():
+            for m in range(messages):
+                message(q, m).wait_send()
+
     for c in range(chunks):
         mixed = snd_o[c, t].astype(F32)
         for k in range(1, n_tp):
@@ -460,7 +539,7 @@
     heads = decay_rate.shape[1]
     both = 2 * inner
     rows = n_tp * own_rows
-    state_rows = STATE // n_sp
+    messages = 2 * (inner // LANES)
     chunk = width // n_tp
     vmem = pl.BlockSpec(memory_space=pltpu.VMEM)
     anywhere = pl.BlockSpec(memory_space=pl.ANY)
@@ -482,11 +561,11 @@
         pltpu.VMEM((n_tp, 8, cols), F32),
         pltpu.VMEM((4, 1, width), F32),
         pltpu.VMEM((rows + PAD + ctx_rows, width), BF16),
-        pltpu.VMEM((n_sp, state_rows, 2 * both), BF16),
-        pltpu.VMEM((n_sp, state_rows, 2 * both), BF16),
-        pltpu.VMEM((n_sp, 8, both), F32),
-        pltpu.VMEM((n_sp, state_rows, both), BF16),
-        pltpu.VMEM((n_sp, state_rows, both), BF16),
+        pltpu.VMEM((2, messages, STATE, LANES), F32),
+        pltpu.VMEM((2, messages, 8, LANES), F32),
+        pltpu.VMEM((2, messages, STATE, LANES), BF16),
+        pltpu.VMEM((2, messages, STATE, LANES), BF16),
+        pltpu.VMEM((n_sp, 8, LANES), F32),
         pltpu.VMEM((n_tp, n_tp, own_rows, chunk), BF16),
         pltpu.VMEM((n_tp, n_tp, own_rows, chunk), BF16),
         dma((9,)),
@@ -500,10 +579,8 @@
         dma((n_tp,)),
         dma((2 + 2 * n_tp,)),
         dma((4,)),
-        dma((n_sp,)),
-        dma((n_sp,)),
-        dma((n_sp,)),
-        dma((n_sp,)),
+        dma((2, messages)),
+        dma((2, messages)),
         dma((n_sp,)),
         dma((n_sp,)),
         dma((n_tp * n_tp,)),
@@ -516,7 +593,7 @@
         out_specs=vmem,
         scratch_shapes=scratch,
         compiler_params=pltpu.CompilerParams(
-            has_side_effects=True, vmem_limit_bytes=62_000_000
+            has_side_effects=True, collective_id=0, vmem_limit_bytes=62_000_000
         ),
     )(
         condition,

time: 53.1 us -> 44.5 us (0.84)
  Pallas kernels: 51.3 us -> 42.7 us
    pallas_call x1, Pallas kernels: 51.3 us -> 42.7 us  [shards(): pl.pallas_call(functools.partial(kernel, n_sp, n_tp, n_dp, heads), out_sh...]
where the time goes in v3:
time: 44.5 us; the launch traced here: 44.3 us
  Pallas kernels  42.7 us (96%)
  local copies, waits for them, and re-layouts  1.57 us (4%)
    pallas_call x1, Pallas kernels, shards(): pl.pallas_call(functools.partial(kernel, n_sp, n_tp, n_dp, heads), out_sh...  42.7 us
    unnamed x1, local copies, waits for them, and re-layouts  1.57 us

profile of v3, /device:TPU:0, one launch (start us, length us, event | category | flops | bytes accessed | tf_op | source)
XLA Modules:
  0.0 44.3 jit_solution(10312485286810100045)
XLA Ops:
  0.0 42.7 %shard_map.163 = bf16[32,2048]{1,0:T(8,128)(2,1)} custom-call(bf16[1,2048]{1,0:T(2,128)(2,1)} %condition.1, bf16[2048]{0:T(1024)(128)(2,1)} %source.1, bf16[2048]{0:T(1024)(128)(2,1)} %gain.1, bf16[3,512]{1,0:T(4,128)(2,1)} %conv_x.1, bf16[3,128]{1,0:T(4,128)(2,1)} %conv_b.1, bf16[3,128]{1,0:T(4,128)(2,1)} %conv_c.1, f32[2,8]{1,0:T(2,128)} %rate.1, ...), custom_call_target="tpu_custom_call" | custom-call | tf_op jit(solution)/shard_map/pallas_call | solution.py:589
  42.7 1.6 %copy.19 = bf16[1,32,2048]{2,1,0:T(8,128)(2,1)} copy(bf16[1,32,2048]{2,1,0:T(8,128)(2,1)} %bitcast.5) | data formatting | bytes 262144

commit v4 on v3

--- a/solution.py
+++ b/solution.py
@@ -355,6 +355,10 @@
     l_moved = moved(x_in, l_steps)
     l_scaled = (l_moved.astype(F32) * expand(jnp.exp(l_ends - l_sums))).astype(BF16)
     l_state = dot(b_in, l_scaled, ((0,), (0,)))
+    pc = project(wc, rows + PAD)
+    c_in = shaped(pc[0:rows], pc[rows : rows + 1], pc[rows + 1 : rows + 2], conv_c)
+    scores = dot(c_in, b_in, ((1,), (1,)))
+    gate = silu(project(wz, rows))
     for copy in t_moves:
         copy.wait()
     row_lane = lax.broadcasted_iota(jnp.int32, (1, LANES), 1)
@@ -422,9 +426,6 @@
         for m in range(messages):
             hop(near, m)
 
-    pc = project(wc, rows + PAD)
-    c_in = shaped(pc[0:rows], pc[rows : rows + 1], pc[rows + 1 : rows + 2], conv_c)
-    scores = dot(c_in, b_in, ((1,), (1,)))
     at_t = lax.broadcasted_iota(jnp.int32, (rows, rows), 0)
     at_s = lax.broadcasted_iota(jnp.int32, (rows, rows), 1)
     sums_t = jnp.transpose(l_sums)
@@ -449,7 +450,6 @@
         inside.append(value)
     inside = jnp.concatenate(inside, axis=1)
     growth = expand(jnp.exp(l_sums))
-    gate = silu(project(wz, rows))
 
     lag = messages // 2
 

time: 44.5 us -> 44.5 us (level)
  no operation moved by 1% of the time
where the time goes in v4:
time: 44.5 us; the launch traced here: 44.4 us
  Pallas kernels  42.8 us (96%)
  local copies, waits for them, and re-layouts  1.57 us (4%)
    pallas_call x1, Pallas kernels, shards(): pl.pallas_call(functools.partial(kernel, n_sp, n_tp, n_dp, heads), out_sh...  42.8 us
    unnamed x1, local copies, waits for them, and re-layouts  1.57 us

profile of v4, /device:TPU:0, one launch (start us, length us, event | category | flops | bytes accessed | tf_op | source)
XLA Modules:
  0.0 44.4 jit_solution(16640625401067070086)
XLA Ops:
  0.0 42.8 %shard_map.163 = bf16[32,2048]{1,0:T(8,128)(2,1)} custom-call(bf16[1,2048]{1,0:T(2,128)(2,1)} %condition.1, bf16[2048]{0:T(1024)(128)(2,1)} %source.1, bf16[2048]{0:T(1024)(128)(2,1)} %gain.1, bf16[3,512]{1,0:T(4,128)(2,1)} %conv_x.1, bf16[3,128]{1,0:T(4,128)(2,1)} %conv_b.1, bf16[3,128]{1,0:T(4,128)(2,1)} %conv_c.1, f32[2,8]{1,0:T(2,128)} %rate.1, ...), custom_call_target="tpu_custom_call" | custom-call | tf_op jit(solution)/shard_map/pallas_call | solution.py:589
  42.8 1.6 %copy.19 = bf16[1,32,2048]{2,1,0:T(8,128)(2,1)} copy(bf16[1,32,2048]{2,1,0:T(8,128)(2,1)} %bitcast.5) | data formatting | bytes 262144
